TPU v7x, 32 devices: a whole 2x2x4 slice. The times are simulated.
32 devices in a mesh: ep: 32 (over z, y, x, core).
Axes of the slice: x: 2, y: 2, z: 4, core: 2. Of those that a mesh axis runs over, the one named last changes fastest.
Arguments:
- tokens: bfloat16 [768, 2048], P('ep'), may hold values from -6 to 6
- state: float32 [768, 16, 64, 64], P('ep'), may hold values from -4 to 4
- norm_gain: float32 [2048], replicated, may hold values from 0.1 to 1.9
- w_recept: bfloat16 [2048, 1024], replicated, may hold values from -0.125 to 0.125
- w_keys: bfloat16 [2048, 1024], replicated, may hold values from -0.125 to 0.125
- w_values: bfloat16 [2048, 1024], replicated, may hold values from -0.125 to 0.125
- decay_base: float32 [1024], replicated, may hold values from -3 to 3
- decay_first_matrix: bfloat16 [2048, 128], replicated, may hold values from -0.125 to 0.125
- decay_second_matrix: bfloat16 [128, 1024], replicated, may hold values from -0.5 to 0.5
- rate_base: float32 [1024], replicated, may hold values from -3 to 3
- rate_first_matrix: bfloat16 [2048, 128], replicated, may hold values from -0.125 to 0.125
- rate_second_matrix: bfloat16 [128, 1024], replicated, may hold values from -0.5 to 0.5
- head_gain: float32 [1024], replicated, may hold values from 0.1 to 1.9
- w_output: bfloat16 [1024, 2048], replicated, may hold values from -0.1875 to 0.1875
- second_gain: float32 [2048], replicated, may hold values from 0.1 to 1.9
- route_ids: int32 [768, 2], replicated, may hold values from 0 to 15, all different within a row; in each aligned block of 24 rows (0 to 23, 24 to 47, ...) at most 6 rows name the same one
- route_weights: float32 [768, 2], replicated, may hold values from 0.2 to 1
- expert_gate: bfloat16 [2048, 49152], P(None, 'ep'), may hold values from -0.125 to 0.125
- expert_up: bfloat16 [2048, 49152], P(None, 'ep'), may hold values from -0.125 to 0.125
- expert_down: bfloat16 [49152, 2048], P('ep'), may hold values from -0.109375 to 0.109375
Outputs:
- layer_out: bfloat16 [768, 2048], P('ep')
- new_state: float32 [768, 16, 64, 64], P('ep')
Inputs may be any that keep to these rules, and one draw needn't show every extreme that they name: `route_ids`: each row names 2 different experts. Among the 24 rows of one device (aligned blocks), no expert is named by more than 6 rows, and in every draw some block names some expert exactly 6 times.
All inputs are finite; a program needn't handle non-finite values.
Results may differ from a plain program's by a relative error of at most 0.015.
Values may be sent and summed in bfloat16 or wider, within the bound.
No kernel may reach another device: no remote copies, remote signals or barrier semaphores. Data moves between devices by JAX's collectives and lax.ppermute only.
A program may use at most 192 MiB of HBM per device.

v0:
```python
import jax
import jax.numpy as jnp
from jax import lax
from jax.sharding import PartitionSpec as P

EXPERTS = 16
CAP_DEV = 6


def norm_rows(values, gain):
    mean_sq = jnp.mean(values * values, axis=-1, keepdims=True)
    return values * lax.rsqrt(mean_sq + 1e-06) * gain


def time_mixer(
    tokens,
    state,
    norm_gain,
    w_recept,
    w_keys,
    w_values,
    decay_base,
    decay_first_matrix,
    decay_second_matrix,
    rate_base,
    rate_first_matrix,
    rate_second_matrix,
    head_gain,
    w_output,
):
    count = tokens.shape[0]
    heads = state.shape[1]
    width = state.shape[2]
    resid = tokens.astype(jnp.float32)
    normed = norm_rows(resid, norm_gain).astype(jnp.bfloat16)
    recept = jnp.dot(normed, w_recept, preferred_element_type=jnp.float32).astype(jnp.bfloat16)
    keys = jnp.dot(normed, w_keys, preferred_element_type=jnp.float32).astype(jnp.bfloat16)
    vals = jnp.dot(normed, w_values, preferred_element_type=jnp.float32).astype(jnp.bfloat16)
    decay_low = jnp.tanh(
        jnp.dot(normed, decay_first_matrix, preferred_element_type=jnp.float32)
    ).astype(jnp.bfloat16)
    rate_low = jnp.dot(normed, rate_first_matrix, preferred_element_type=jnp.float32).astype(
        jnp.bfloat16
    )
    pre = decay_base + jnp.dot(decay_low, decay_second_matrix, preferred_element_type=jnp.float32)
    decay = jnp.exp(-jnp.exp(-jax.nn.softplus(-pre) - 0.5))
    rate = jax.nn.sigmoid(
        rate_base + jnp.dot(rate_low, rate_second_matrix, preferred_element_type=jnp.float32)
    )

    def split_heads(values):
        return values.astype(jnp.float32).reshape(count, heads, width)

    r_head = split_heads(recept)
    k_head = split_heads(keys)
    v_head = split_heads(vals)
    d_head = split_heads(decay)
    a_head = split_heads(rate)
    unit = k_head * lax.rsqrt(jnp.sum(k_head * k_head, axis=-1, keepdims=True) + 1e-06)
    probe = jnp.einsum("bhvk,bhk->bhv", state, unit, precision=lax.Precision.HIGHEST)
    updated = (
        state * d_head[:, :, None, :]
        - probe[..., None] * (unit * a_head)[:, :, None, :]
        + v_head[..., None] * k_head[:, :, None, :]
    )
    mixed = jnp.einsum("bhvk,bhk->bhv", updated, r_head, precision=lax.Precision.HIGHEST)
    centre = mixed - jnp.mean(mixed, axis=-1, keepdims=True)
    spread = jnp.mean(centre * centre, axis=-1, keepdims=True)
    mixed = centre * lax.rsqrt(spread + 0.00064)
    mixed = (mixed.reshape(count, heads * width) * head_gain).astype(jnp.bfloat16)
    after = resid + jnp.dot(mixed, w_output, preferred_element_type=jnp.float32)
    return (after, updated)


def expert_part(rows, gate_w, up_w, down_w):
    gate = jnp.dot(rows, gate_w, preferred_element_type=jnp.float32)
    upper = jnp.dot(rows, up_w, preferred_element_type=jnp.float32)
    hidden = (jax.nn.silu(gate) * upper).astype(jnp.bfloat16)
    return jnp.dot(hidden, down_w, preferred_element_type=jnp.float32)


def slot_table(member, slots):
    order = jnp.cumsum(member.astype(jnp.int32), axis=1) - 1
    match = order[:, None, :] == jnp.arange(slots, dtype=jnp.int32)[None, :, None]
    return (match & member[:, None, :]).astype(jnp.float32)


def on_device(
    tokens,
    state,
    norm_gain,
    w_recept,
    w_keys,
    w_values,
    decay_base,
    decay_first_matrix,
    decay_second_matrix,
    rate_base,
    rate_first_matrix,
    rate_second_matrix,
    head_gain,
    w_output,
    second_gain,
    route_ids,
    route_weights,
    expert_gate,
    expert_up,
    expert_down,
):
    after, new_state = time_mixer(
        tokens,
        state,
        norm_gain,
        w_recept,
        w_keys,
        w_values,
        decay_base,
        decay_first_matrix,
        decay_second_matrix,
        rate_base,
        rate_first_matrix,
        rate_second_matrix,
        head_gain,
        w_output,
    )
    second = norm_rows(after, second_gain).astype(jnp.bfloat16)
    devices = lax.axis_size("ep")
    group = devices // EXPERTS
    rows_dev = tokens.shape[0]
    slots = CAP_DEV
    width = tokens.shape[1]
    start = lax.axis_index("ep") * rows_dev
    own_ids = lax.dynamic_slice_in_dim(route_ids, start, rows_dev, 0)
    own_weights = lax.dynamic_slice_in_dim(route_weights, start, rows_dev, 0)
    hit = own_ids[None, :, :] == jnp.arange(EXPERTS, dtype=jnp.int32)[:, None, None]
    member = jnp.any(hit, axis=2)
    share = jnp.sum(jnp.where(hit, own_weights[None, :, :], 0.0), axis=2)
    table = slot_table(member, slots)
    packed = jnp.einsum(
        "ecs,sf->ecf", table.astype(jnp.bfloat16), second, preferred_element_type=jnp.float32
    ).astype(jnp.bfloat16)
    outgoing = jnp.repeat(packed, group, axis=0)
    received = lax.all_to_all(outgoing, "ep", split_axis=0, concat_axis=0, tiled=True)
    count = received.shape[1]
    partial_value = expert_part(
        received.reshape(devices * count, width), expert_gate, expert_up, expert_down
    )
    returned = lax.all_to_all(
        partial_value.reshape(devices, count, width).astype(jnp.bfloat16),
        "ep",
        split_axis=0,
        concat_axis=0,
        tiled=True,
    ).astype(jnp.float32)
    summed = jnp.sum(returned.reshape(EXPERTS, group, slots, width), axis=1)
    blend = jnp.einsum(
        "ecs,ecf->sf", table * share[:, None, :], summed, precision=lax.Precision.HIGHEST
    )
    layer_out = (after + blend).astype(jnp.bfloat16)
    return (layer_out, new_state)


def solution(mesh):
    in_specs = (
        P("ep", None),
        P("ep", None, None, None),
        P(),
        P(),
        P(),
        P(),
        P(),
        P(),
        P(),
        P(),
        P(),
        P(),
        P(),
        P(),
        P(),
        P(),
        P(),
        P(None, "ep"),
        P(None, "ep"),
        P("ep", None),
    )
    out_specs = (P("ep", None), P("ep", None, None, None))
    return jax.shard_map(
        on_device, mesh=mesh, in_specs=in_specs, out_specs=out_specs, check_vma=False
    )
```

profile of v0, /device:TPU:0, one launch (start us, length us, event | category | flops | bytes accessed | tf_op | source)
XLA Modules:
  0.0 139.8 jit_solution(11655732401048659084)
XLA Ops:
  0.6 0.0 copy-start
  0.6 0.0 copy-start.3
  0.7 0.0 copy-start.6
  0.7 0.0 copy-start.8
  0.7 0.0 copy-start.4
  0.7 0.0 copy-start.5
  0.7 1.1 fusion.13
  1.8 3.0 %fusion.9 = f32[24,1024]{1,0:T(8,128)S(1)} fusion(bf16[2048,1024]{1,0:T(8,128)(2,1)} %param.24, bf16[24,2048]{1,0:T(8,128)(2,1)} %param.20, f32[2048]{0:T(1024)} %param.22, f32[24]{0:T(128)S(1)} %add_rsqrt_fusion.3), kind=kOutput, calls=%fused_computation.21 | convolution fusion | flops 100909056 | bytes 4399200 | tf_op jit(solution)/shard_map/dot_general | solution.py:37
  4.8 0.1 reshape.109
  4.9 0.1 multiply_reduce_fusion.2
  5.1 0.0 copy-done
  5.1 1.4 %fusion.7 = f32[24,1024]{1,0:T(8,128)S(1)} fusion(bf16[128,1024]{1,0:T(8,128)(2,1)} %param.31, bf16[2048,128]{1,0:T(8,128)(2,1)S(1)} %copy-done, f32[1024]{0:T(1024)} %param.29, bf16[24,2048]{1,0:T(8,128)(2,1)} %param.20, f32[2048]{0:T(1024)} %param.22, f32[24]{0:T(128)S(1)} %add_rsqrt_fusion.3), kind=kOutput, calls=%fused_computation.16 | convolution fusion | flops 19172352 | bytes 995424 | tf_op jit(solution)/shard_map/dot_general | solution.py:48
  6.5 0.1 reshape.101
  6.6 0.0 copy-done.3
  6.6 0.0 copy-done.6
  6.6 0.0 copy-done.8
  6.6 0.0 copy-done.4
  6.6 0.0 copy-done.5
  6.6 0.5 fusion.22
  7.1 0.1 mul.143
  7.2 2.9 %fusion.8 = f32[24,1024]{1,0:T(8,128)S(1)} fusion(bf16[2048,1024]{1,0:T(8,128)(2,1)} %param.25, bf16[24,2048]{1,0:T(8,128)(2,1)S(1)} %copy-done.3, f32[2048]{0:T(1024)S(1)} %copy-done.6, f32[24]{0:T(128)S(1)} %add_rsqrt_fusion.3), kind=kOutput, calls=%fused_computation.19 | convolution fusion | flops 100909056 | bytes 4399200 | tf_op jit(solution)/shard_map/dot_general | solution.py:38
  10.1 0.1 reshape.110
  10.2 2.9 %convolution_convert_fusion.2 = bf16[24,1024]{1,0:T(8,128)(2,1)S(1)} fusion(bf16[2048,1024]{1,0:T(8,128)(2,1)} %param.23, bf16[24,2048]{1,0:T(8,128)(2,1)S(1)} %copy-done.3, f32[2048]{0:T(1024)S(1)} %copy-done.6, f32[24]{0:T(128)S(1)} %add_rsqrt_fusion.3), kind=kOutput, calls=%fused_computation.17 | convolution fusion | flops 100884480 | bytes 4350048 | tf_op jit(solution)/shard_map/dot_general | solution.py:36
  13.1 0.2 reshape.120
  13.2 0.1 fusion.45
  13.4 22.0 %fusion.46 = f32[24,16,1,64]{3,2,1,0:T(1,128)S(1)} fusion(f32[24,16,64,1]{2,3,1,0:T(1,128)S(1)} %bitcast.42, f32[24,16,64,64]{3,2,1,0:T(8,128)} %param.21), kind=kOutput, calls=%fused_computation.73 | convolution fusion | flops 18874368 | bytes 6488064 | tf_op jit(solution)/shard_map/bhvk,bhk->bhv/dot_general | solution.py:60
  35.4 9.8 %multiply_add_fusion = f32[24,16,64,64]{3,2,1,0:T(8,128)S(1)} fusion(f32[24,16,64,64]{3,2,1,0:T(8,128)} %param.21, f32[24,16,64]{2,1,0:T(8,128)S(1)} %reshape.109, f32[24,16,64]{2,1,0:T(8,128)S(1)} %reshape.110, f32[24,16,64]{2,1,0:T(8,128)S(1)} %get-tuple-element.2, f32[24,16,64]{2,1,0:T(8,128)S(1)} %bitcast.41, f32[24,16,64]{2,1,0:T(8,128)S(1)} %mul.143), kind=kLoop, calls=%fused_computation | loop fusion | flops 7864320 | bytes 13074432 | tf_op jit(solution)/shard_map/add | solution.py:62
  45.2 0.0 copy-start.2
  45.3 0.0 copy-start.9
  45.3 0.0 copy-start.7
  45.3 9.9 %fusion.47 = f32[24,16,1,64]{3,2,1,0:T(1,128)S(1)} fusion(f32[24,16,64,64]{3,2,1,0:T(8,128)S(1)} %multiply_add_fusion, bf16[24,16,64,1]{2,3,1,0:T(2,128)(2,1)S(1)} %reshape.120), kind=kOutput, calls=%fused_computation.74 | convolution fusion | flops 18874368 | bytes 6438912 | tf_op jit(solution)/shard_map/bhvk,bhk->bhv/dot_general | solution.py:66
  55.1 0.0 copy-done.2
  55.1 0.1 reduce_sum.65
  55.3 0.2 multiply_reduce_fusion.1
  55.5 0.2 subtract_multiply_fusion
  55.7 0.1 reshape.103
  55.8 0.0 copy-done.9
  55.8 3.0 %multiply_reduce_fusion = (f32[24]{0:T(128)S(1)}, f32[24,2048]{1,0:T(8,128)S(1)}) fusion(bf16[1024,2048]{1,0:T(8,128)(2,1)} %param.33, f32[24,1024]{1,0:T(8,128)S(1)} %reshape.103, f32[1024]{0:T(1024)S(1)} %copy-done.9, bf16[24,2048]{1,0:T(8,128)(2,1)S(1)} %copy-done.3), kind=kOutput, calls=%fused_computation.34 | convolution fusion | flops 100909032 | bytes 4591712 | tf_op jit(solution)/shard_map/dot_general | solution.py:71
  58.8 0.8 constant_dynamic-slice_fusion.1
  59.6 0.2 reduce_window_sum.11
  59.8 0.0 copy-done.7
  59.8 0.3 convolution_convert_fusion.1
  60.1 0.2 copy.32
  60.3 0.1 broadcast_in_dim.12
  60.4 33.3 %all_to_all.10 = bf16[32,6,2048]{2,1,0:T(8,128)(2,1)S(1)} all-to-all(bf16[32,6,2048]{2,1,0:T(8,128)(2,1)S(1)} %bitcast.37), channel_id=1, replica_groups=mesh['ep'=32] {'ep'}, dimensions={0} | all-to-all | bytes 1572864 | tf_op jit(solution)/shard_map/all_to_all | solution.py:143
  93.8 0.3 reshape.105
  94.0 5.2 %fusion.48 = f32[192,1536]{1,0:T(8,128)} fusion(bf16[192,2048]{1,0:T(8,128)(2,1)S(1)} %reshape.105, bf16[2048,1536]{1,0:T(8,128)(2,1)} %param.37), kind=kOutput, calls=%fused_computation.75 | convolution fusion | flops 1207959552 | bytes 8257536 | tf_op jit(solution)/shard_map/dot_general | solution.py:76
  99.2 0.0 copy-start.1
  99.2 7.7 %convolution_convert_fusion = bf16[192,2048]{1,0:T(8,128)(2,1)S(1)} fusion(bf16[1536,2048]{1,0:T(8,128)(2,1)} %param.39, bf16[192,2048]{1,0:T(8,128)(2,1)S(1)} %reshape.105, bf16[2048,1536]{1,0:T(8,128)(2,1)} %param.38, f32[192,1536]{1,0:T(8,128)} %fusion.48), kind=kOutput, calls=%fused_computation.3 | convolution fusion | flops 2418081792 | bytes 15335424 | tf_op jit(solution)/shard_map/dot_general | solution.py:79
  106.9 1.2 convert_element_type.74
  108.1 3.6 %all-to-all-start.1 = ((bf16[32,6,2048]{2,1,0:T(8,128)(2,1)}), bf16[32,6,2048]{2,1,0:T(8,128)(2,1)S(1)}, u32[]{:S(2)}, u32[]{:S(2)}) async-start(bf16[32,6,2048]{2,1,0:T(8,128)(2,1)} %convert_element_type.74), calls=%async_computation.1 | async-start | bytes 2097152 | tf_op jit(solution)/shard_map/all_to_all | solution.py:148
  111.8 0.8 constant_dynamic-slice_fusion
  112.6 25.4 %all-to-all-done.1 = bf16[32,6,2048]{2,1,0:T(8,128)(2,1)S(1)} async-done(((bf16[32,6,2048]{2,1,0:T(8,128)(2,1)}), bf16[32,6,2048]{2,1,0:T(8,128)(2,1)S(1)}, u32[]{:S(2)}, u32[]{:S(2)}) %all-to-all-start.1) | async-done | bytes 786464 | tf_op jit(solution)/shard_map/all_to_all | solution.py:148
  138.0 0.2 convert_reduce_fusion
  138.2 1.6 %fusion.2 = bf16[24,2048]{1,0:T(8,128)(2,1)} fusion(f32[24,2048]{1,0:T(8,128)S(1)} %get-tuple-element.5, f32[16,6,2048]{2,1,0:T(8,128)S(1)} %convert_reduce_fusion, f32[16,24]{1,0:T(8,128)S(1)} %select_reduce_fusion, s32[16,24]{1,0:T(8,128)S(1)} %broadcast_add_fusion, pred[16,24]{1,0:T(8,128)(4,1)S(1)} %fusion.35), kind=kOutput, calls=%fused_computation.8 | convolution fusion | flops 56728320 | bytes 1084800 | tf_op jit(solution)/shard_map/ecs,ecf->sf/dot_general | solution.py:156
  139.8 0.0 copy-done.1
  (9 shorter events, 0.1 us)
Async XLA Ops:
  0.6 4.4 %copy-start = (bf16[2048,128]{1,0:T(8,128)(2,1)S(1)}, bf16[2048,128]{1,0:T(8,128)(2,1)}, u32[]{:S(2)}) copy-start(bf16[2048,128]{1,0:T(8,128)(2,1)} %param.30) | copy-start | bytes 1572868
  0.6 5.9 %copy-start.3 = (bf16[24,2048]{1,0:T(8,128)(2,1)S(1)}, bf16[24,2048]{1,0:T(8,128)(2,1)}, u32[]{:S(2)}) copy-start(bf16[24,2048]{1,0:T(8,128)(2,1)} %param.20) | copy-start | bytes 294916
  0.7 5.9 %copy-start.6 = (f32[2048]{0:T(1024)S(1)}, f32[2048]{0:T(1024)}, u32[]{:S(2)}) copy-start(f32[2048]{0:T(1024)} %param.22) | copy-start | bytes 24580
  0.7 5.9 %copy-start.8 = (f32[1024]{0:T(1024)S(1)}, f32[1024]{0:T(1024)}, u32[]{:S(2)}) copy-start(f32[1024]{0:T(1024)} %param.26) | copy-start | bytes 12292
  0.7 5.9 %copy-start.4 = (bf16[2048,128]{1,0:T(8,128)(2,1)S(1)}, bf16[2048,128]{1,0:T(8,128)(2,1)}, u32[]{:S(2)}) copy-start(bf16[2048,128]{1,0:T(8,128)(2,1)} %param.27) | copy-start | bytes 1572868
  0.7 5.9 %copy-start.5 = (bf16[128,1024]{1,0:T(8,128)(2,1)S(1)}, bf16[128,1024]{1,0:T(8,128)(2,1)}, u32[]{:S(2)}) copy-start(bf16[128,1024]{1,0:T(8,128)(2,1)} %param.28) | copy-start | bytes 786436
  45.2 9.9 %copy-start.2 = (f32[24,16,64,64]{3,2,1,0:T(8,128)}, f32[24,16,64,64]{3,2,1,0:T(8,128)S(1)}, u32[]{:S(2)}) copy-start(f32[24,16,64,64]{3,2,1,0:T(8,128)S(1)} %multiply_add_fusion) | copy-start | bytes 18874372
  45.3 10.6 %copy-start.9 = (f32[1024]{0:T(1024)S(1)}, f32[1024]{0:T(1024)}, u32[]{:S(2)}) copy-start(f32[1024]{0:T(1024)} %param.32) | copy-start | bytes 12292
  45.3 14.5 %copy-start.7 = (f32[2048]{0:T(1024)S(1)}, f32[2048]{0:T(1024)}, u32[]{:S(2)}) copy-start(f32[2048]{0:T(1024)} %param.34) | copy-start | bytes 24580
  99.2 40.6 %copy-start.1 = (bf16[2048,128]{1,0:T(8,128)(2,1)S(1)}, bf16[2048,128]{1,0:T(8,128)(2,1)}, u32[]{:S(2)}) copy-start(bf16[2048,128]{1,0:T(8,128)(2,1)} %param.30) | copy-start | bytes 1572868
  108.1 29.8 %all-to-all-start.1 = ((bf16[32,6,2048]{2,1,0:T(8,128)(2,1)}), bf16[32,6,2048]{2,1,0:T(8,128)(2,1)S(1)}, u32[]{:S(2)}, u32[]{:S(2)}) async-start(bf16[32,6,2048]{2,1,0:T(8,128)(2,1)} %convert_element_type.74), calls=%async_computation.1 | async-start | bytes 2097152 | tf_op jit(solution)/shard_map/all_to_all | solution.py:148
where the time goes:
time: 140 us
  matrix products  60.2 us (43%)
  blocking collectives  33.3 us (24%)
  waiting for transfers between devices  25.4 us (18%)
  other arithmetic  12.2 us (9%)
  local copies, waits for them, and re-layouts  4.1 us (3%)
  starting transfers between devices  3.63 us (3%)
    all_to_all x1, blocking collectives, on_device(): lax.all_to_all(outgoing, 'ep', split_axis=0, concat_axis=0, tiled=True)  33.3 us
    all_to_all x1, waiting for transfers between devices, on_device(): lax.all_to_all(partial_value.reshape(devices, count, width).astype(jnp.bf...  25.4 us
    dot_general x1, matrix products, time_mixer(): jnp.einsum('bhvk,bhk->bhv', state, unit, precision=lax.Precision.HIGHEST)  22 us
    dot_general x1, matrix products, time_mixer(): jnp.einsum('bhvk,bhk->bhv', updated, r_head, precision=lax.Precision.HIGH...  9.85 us
    add x1, other arithmetic, time_mixer(): state * d_head[:, :, None, :]  9.85 us
    dot_general x1, matrix products, expert_part(): return jnp.dot(hidden, down_w, preferred_element_type=jnp.float32)  7.66 us
    dot_general x1, matrix products, expert_part(): gate = jnp.dot(rows, gate_w, preferred_element_type=jnp.float32)  5.18 us
    all_to_all x1, starting transfers between devices, on_device(): lax.all_to_all(partial_value.reshape(devices, count, width).astype(jnp.bf...  3.63 us
  transfers between devices with their start and end apart: 1, of which 1 were waited for; matrix products, arithmetic and copies ran while one was open for 1% of the time, Pallas kernels for 0%

commit v1 on v0

v1 whole, which is shorter than its diff:
```python
import functools

import jax
import jax.numpy as jnp
from jax import lax
from jax.experimental import pallas as pl
from jax.experimental.pallas import tpu as pltpu
from jax.sharding import PartitionSpec as P

EXPERTS = 16
CAP_DEV = 6
ROWS = 8
SPLIT = 3

F32 = jnp.float32
BF16 = jnp.bfloat16
HBM = pl.BlockSpec(memory_space=pltpu.HBM)
VMEM = pl.BlockSpec(memory_space=pltpu.VMEM)
SMEM = pl.BlockSpec(memory_space=pltpu.SMEM)


def pin(value):
    return pltpu.with_memory_space_constraint(value, pltpu.HBM)


def iota(shape, dim):
    return lax.broadcasted_iota(jnp.int32, shape, dim)


def dot(a, b):
    return jnp.dot(a, b, preferred_element_type=F32)


def dot_t(a, b):
    return lax.dot_general(a, b, (((0,), (0,)), ((), ())), preferred_element_type=F32)


def head_sums(x):
    low = iota(x.shape, 1) < 64
    first = jnp.sum(jnp.where(low, x, 0.0), axis=1, keepdims=True)
    other = jnp.sum(jnp.where(low, 0.0, x), axis=1, keepdims=True)
    return jnp.where(low, first, other)


def mixer_kernel(
    start,
    tokens_in,
    norm_gain_in,
    decay_base_in,
    rate_base_in,
    head_gain_in,
    second_gain_in,
    ids_in,
    weights_in,
    state,
    w_recept,
    w_keys,
    w_values,
    decay_first,
    decay_second,
    rate_first,
    rate_second,
    w_output,
    packed,
    after_out,
    combine,
    terms_out,
    s_buf,
    wr_buf,
    wk_buf,
    wv_buf,
    d1_buf,
    d2_buf,
    r1_buf,
    r2_buf,
    wo_buf,
    lhs_buf,
    sums,
    tokens,
    norm_gain,
    decay_base,
    rate_base,
    head_gain,
    second_gain,
    ids_t,
    weights_t,
    w_sem,
    s_sem,
    a_sem,
):
    keys_out, vals_out, decay_out, ua_out, probe_out = (terms_out.at[i] for i in range(5))
    rows, width = tokens.shape
    small = [
        pltpu.make_async_copy(src, dst, a_sem.at[i])
        for i, (src, dst) in enumerate(
            (
                (tokens_in, tokens),
                (norm_gain_in, norm_gain),
                (ids_in, ids_t),
                (weights_in, weights_t),
                (decay_base_in, decay_base),
                (rate_base_in, rate_base),
                (head_gain_in, head_gain),
                (second_gain_in, second_gain),
            )
        )
    ]
    for copy in small:
        copy.start()
    heads = state.shape[1]
    chan = heads * 64
    groups = s_sem.shape[0]
    step = heads // groups
    pairs = heads // 2

    def weight(i, src, dst):
        return pltpu.make_async_copy(src, dst, w_sem.at[i])

    def state_copy(g):
        return pltpu.make_async_copy(
            state.at[:, pl.ds(g * step, step)], s_buf.at[:, pl.ds(g * step, step)], s_sem.at[g]
        )

    k_copy = weight(0, w_keys, wk_buf)
    d1_copy = weight(1, decay_first, d1_buf)
    r1_copy = weight(2, rate_first, r1_buf)
    d2_copy = weight(3, decay_second, d2_buf)
    r2_copy = weight(4, rate_second, r2_buf)
    r_copy = weight(5, w_recept, wr_buf)
    v_copy = weight(6, w_values, wv_buf)
    half = chan // 2
    o_copies = [
        weight(7 + i, w_output.at[pl.ds(i * half, half)], wo_buf.at[pl.ds(i * half, half)])
        for i in range(2)
    ]
    for copy in (k_copy, d1_copy, r1_copy, d2_copy, r2_copy, r_copy):
        copy.start()

    for copy in small:
        copy.wait()

    all_rows = ids_t.shape[1]
    pick = (iota((all_rows, rows), 0) == iota((all_rows, rows), 1) + start[0]).astype(F32)
    own_ids = jnp.dot(ids_t[...].astype(F32), pick, preferred_element_type=F32)
    own_weights = jnp.dot(
        weights_t[...], pick, preferred_element_type=F32, precision=lax.Precision.HIGHEST
    )
    expert = iota((EXPERTS, rows), 0).astype(F32)
    hit0 = own_ids[0:1] == expert
    hit1 = own_ids[1:2] == expert
    member = jnp.where(hit0 | hit1, 1.0, 0.0)
    share = jnp.where(hit0, own_weights[0:1], 0.0) + jnp.where(hit1, own_weights[1:2], 0.0)
    before = (iota((rows, rows), 0) < iota((rows, rows), 1)).astype(F32)
    order = dot(member, before)
    spread = (iota((EXPERTS * ROWS, EXPERTS), 0) // ROWS == iota((EXPERTS * ROWS, EXPERTS), 1))
    spread = spread.astype(F32)
    member_r = dot(spread, member) > 0.5
    order_r = dot(spread, order).astype(jnp.int32)
    share_r = jnp.dot(spread, share, preferred_element_type=F32, precision=lax.Precision.HIGHEST)
    row = iota((EXPERTS * ROWS, rows), 0) % ROWS
    tables = [jnp.where(member_r & (row < CAP_DEV) & (order_r == row), 1.0, 0.0)]
    for j in range(SPLIT):
        slot = SPLIT * (row - CAP_DEV) + j
        tables.append(jnp.where(member_r & (row >= CAP_DEV) & (order_r == slot), 1.0, 0.0))
    for j in range(SPLIT + 1):
        combine[j] = tables[j] * share_r

    resid = tokens[...].astype(F32)
    mean_sq = jnp.mean(resid * resid, axis=1, keepdims=True)
    normed = (resid * lax.rsqrt(mean_sq + 1e-06) * norm_gain[...]).astype(BF16)

    k_copy.wait()
    state_copy(0).start()
    keys_out[...] = dot(normed, wk_buf[...]).astype(BF16).astype(F32)
    d1_copy.wait()
    decay_low = jnp.tanh(dot(normed, d1_buf[...])).astype(BF16)
    r1_copy.wait()
    state_copy(1).start()
    rate_low = dot(normed, r1_buf[...]).astype(BF16)
    d2_copy.wait()
    pre = decay_base[...] + dot(decay_low, d2_buf[...])
    decay_out[...] = jnp.exp(-jnp.exp(-jax.nn.softplus(-pre) - 0.5))
    r2_copy.wait()
    rate = jax.nn.sigmoid(rate_base[...] + dot(rate_low, r2_buf[...]))
    r_copy.wait()
    for g in range(2, groups):
        state_copy(g).start()
    v_copy.start()
    recept = dot(normed, wr_buf[...]).astype(BF16).astype(F32)

    for p in range(pairs):
        at = slice(p * 128, p * 128 + 128)
        k = keys_out[:, at]
        unit = k * lax.rsqrt(head_sums(k * k) + 1e-06)
        ua = unit * rate[:, at]
        r = recept[:, at]
        dr = decay_out[:, at] * r
        ua_out[:, at] = ua
        sums[0, :, at] = head_sums(ua * r)
        sums[1, :, at] = head_sums(k * r)
        for h in range(2):
            lanes = slice(h * 64, h * 64 + 64)
            lhs_buf[2 * p + h, 0:rows] = unit[:, lanes]
            lhs_buf[2 * p + h, rows : 2 * rows] = dr[:, lanes]

    own_block = iota((rows, 128), 1) // 64 == iota((rows, 128), 0) % 2
    low = iota((rows, 128), 1) < 64
    token = iota((rows, 128), 0) // 2

    def diagonal(x):
        total = jnp.zeros((rows, 128), F32)
        for c in range(rows * 64 // 128):
            total = total + jnp.where(own_block & (token == c), x[:, c * 128 : c * 128 + 128], 0.0)
        return total + pltpu.roll(total, 64, 1)

    def state_step(g, carry):
        state_copy(g).wait()

        @pl.when(g == 1)
        def _():
            for copy in o_copies:
                copy.start()

        for p in range(step // 2):
            found = []
            for h in range(2):
                head = g * step + 2 * p + h
                block = s_buf[:, head].reshape(rows * 64, 64).astype(BF16)
                found.append(
                    lax.dot_general(
                        lhs_buf[head].astype(BF16),
                        block,
                        (((1,), (1,)), ((), ())),
                        preferred_element_type=F32,
                    )
                )
            at = pl.ds(pl.multiple_of((g * step + 2 * p) * 64, 128), 128)
            probe_out[:, at] = jnp.where(low, diagonal(found[0][:rows]), diagonal(found[1][:rows]))
            sums[2, :, at] = jnp.where(low, diagonal(found[0][rows:]), diagonal(found[1][rows:]))
        return carry

    lax.fori_loop(0, groups, state_step, 0)

    v_copy.wait()
    vals_out[...] = dot(normed, wv_buf[...]).astype(BF16).astype(F32)
    pieces = []
    for p in range(pairs):
        at = slice(p * 128, p * 128 + 128)
        mixed = sums[2, :, at] - probe_out[:, at] * sums[0, :, at] + vals_out[:, at] * sums[1, :, at]
        centre = mixed - head_sums(mixed) * (1.0 / 64)
        var = head_sums(centre * centre) * (1.0 / 64)
        pieces.append((centre * lax.rsqrt(var + 0.00064) * head_gain[:, at]).astype(BF16))
    mixed = jnp.concatenate(pieces, axis=1)
    after = resid
    for i in range(2):
        o_copies[i].wait()
        after = after + dot(mixed[:, i * half : i * half + half], wo_buf[pl.ds(i * half, half)])
    after_out[...] = after
    mean_sq = jnp.mean(after * after, axis=1, keepdims=True)
    second = (after * lax.rsqrt(mean_sq + 1e-06) * second_gain[...]).astype(BF16)
    piece = width // (SPLIT + 1)
    last = second[:, SPLIT * piece :]
    for j in range(SPLIT):
        packed[:, j * piece : (j + 1) * piece] = (
            dot(tables[0].astype(BF16), second[:, j * piece : (j + 1) * piece])
            + dot(tables[1 + j].astype(BF16), last)
        ).astype(BF16)


def mixer(start, args, state, mats):
    rows, width = args[0].shape
    heads = state.shape[1]
    chan = heads * 64
    low = mats[3].shape[1]
    groups = 4
    f = lambda *s: jax.ShapeDtypeStruct(s, F32)
    v = pltpu.VMEM
    return pl.pallas_call(
        mixer_kernel,
        out_shape=(
            jax.ShapeDtypeStruct((EXPERTS * ROWS, width * SPLIT // (SPLIT + 1)), BF16),
            f(rows, width),
            f(SPLIT + 1, EXPERTS * ROWS, rows),
            f(5, rows, chan),
        ),
        in_specs=[SMEM] + [HBM] * (len(args) + 1 + len(mats)),
        out_specs=(VMEM,) * 4,
        scratch_shapes=[
            v(state.shape, F32),
            v((width, chan), BF16),
            v((width, chan), BF16),
            v((width, chan), BF16),
            v((width, low), BF16),
            v((low, chan), BF16),
            v((width, low), BF16),
            v((low, chan), BF16),
            v((chan, width), BF16),
            v((heads, 2 * rows, 64), F32),
            v((3, rows, chan), F32),
            *(v(a.shape, a.dtype) for a in args),
            pltpu.SemaphoreType.DMA((9,)),
            pltpu.SemaphoreType.DMA((groups,)),
            pltpu.SemaphoreType.DMA((len(args),)),
        ],
        compiler_params=pltpu.CompilerParams(vmem_limit_bytes=67_000_000),
        cost_estimate=pl.CostEstimate(
            flops=24_000_000_000, bytes_accessed=30_000_000, transcendentals=200_000
        ),
        name="mixer",
    )(start, *map(pin, (*args, state, *mats)))


def update_kernel(
    state,
    terms_in,
    out,
    buf,
    lhs,
    in_sem,
    out_sem,
    terms,
    t_sem,
):
    keys, vals, decay, ua, probe = (terms.at[i] for i in range(5))
    terms_copy = pltpu.make_async_copy(terms_in, terms, t_sem.at[0])
    terms_copy.start()
    rows, heads = buf.shape[0], buf.shape[1]
    pairs = heads // 2

    def load(p):
        at = pl.ds(p * 2, 2)
        return pltpu.make_async_copy(state.at[:, at], buf.at[:, at], in_sem.at[p])

    def store(p):
        at = pl.ds(p * 2, 2)
        return pltpu.make_async_copy(buf.at[:, at], out.at[:, at], out_sem.at[p])

    for p in range(pairs):
        load(p).start()

    column = iota((64, 4 * rows), 1) % rows
    terms_copy.wait()

    def body(p, carry):
        lanes = pl.ds(pl.multiple_of(p * 128, 128), 128)
        d = decay[:, lanes]
        u, q = ua[:, lanes], probe[:, lanes]
        u_high = u.astype(BF16).astype(F32)
        q_high = q.astype(BF16).astype(F32)
        left = jnp.concatenate([vals[:, lanes], q_high, q - q_high, q_high], axis=0).T
        right = jnp.concatenate([keys[:, lanes], -u_high, -u_high, u_high - u], axis=0)
        load(p).wait()
        for h in range(2):
            part = left[h * 64 : h * 64 + 64]
            for b in range(rows):
                lhs[h, b * 64 : b * 64 + 64] = jnp.where(column == b, part, 0.0).astype(BF16)
            if h:
                right = pltpu.roll(right, 64, 1)
                d = pltpu.roll(d, 64, 1)
            change = dot(lhs[h], right[:, :64].astype(BF16))
            for b in range(rows):
                buf[b, 2 * p + h] = (
                    buf[b, 2 * p + h] * d[b : b + 1, :64] + change[b * 64 : b * 64 + 64]
                )
        store(p).start()
        return carry

    lax.fori_loop(0, pairs, body, 0)
    for p in range(pairs):
        store(p).wait()


def update(state, terms):
    pairs = state.shape[1] // 2
    return pl.pallas_call(
        update_kernel,
        out_shape=jax.ShapeDtypeStruct(state.shape, F32),
        in_specs=[HBM] * 2,
        out_specs=HBM,
        scratch_shapes=[
            pltpu.VMEM(state.shape, F32),
            pltpu.VMEM((2, state.shape[0] * 64, 4 * state.shape[0]), BF16),
            pltpu.SemaphoreType.DMA((pairs,)),
            pltpu.SemaphoreType.DMA((pairs,)),
            pltpu.VMEM(terms.shape, F32),
            pltpu.SemaphoreType.DMA((1,)),
        ],
        compiler_params=pltpu.CompilerParams(vmem_limit_bytes=67_000_000),
        cost_estimate=pl.CostEstimate(
            flops=16_000_000_000, bytes_accessed=26_000_000, transcendentals=0
        ),
        name="update",
    )(pin(state), pin(terms))


def expert_kernel(chunk, group, *refs):
    received = refs[:group]
    gate, up, down = refs[group : group + 3]
    results = refs[group + 3 : 2 * group + 3]
    x_buf, acc = refs[2 * group + 3 :]
    width, hidden = gate.shape
    steps = hidden // chunk
    piece = width // (SPLIT + 1)
    slots = EXPERTS * CAP_DEV
    packed_rows = EXPERTS * ROWS

    source, c = iota((slots, packed_rows), 0) // CAP_DEV, iota((slots, packed_rows), 0) % CAP_DEV
    column = iota((slots, packed_rows), 1)
    tables = [jnp.where(column == source * ROWS + c, 1.0, 0.0).astype(BF16)]
    for j in range(SPLIT):
        here = (column == source * ROWS + CAP_DEV + c // SPLIT) & (c % SPLIT == j)
        tables.append(jnp.where(here, 1.0, 0.0).astype(BF16))
    for m in range(group):
        at = slice(m * slots, (m + 1) * slots)
        value = received[m][...]
        x_buf[at, : SPLIT * piece] = dot(tables[0], value).astype(BF16)
        x_buf[at, SPLIT * piece :] = sum(
            dot(tables[1 + j], value[:, j * piece : (j + 1) * piece]) for j in range(SPLIT)
        ).astype(BF16)

    for i in range(steps):
        at = slice(i * chunk, (i + 1) * chunk)
        x = x_buf[...]
        g = dot(x, gate[:, at])
        u = dot(x, up[:, at])
        h = (jax.nn.silu(g) * u).astype(BF16)
        y = dot(h, down[at])
        acc[...] = y if i == 0 else acc[...] + y

    for m in range(group):
        y = acc[m * slots : (m + 1) * slots].astype(BF16)
        last = y[:, SPLIT * piece :]
        for j in range(SPLIT):
            results[m][:, j * piece : (j + 1) * piece] = (
                dot_t(tables[0], y[:, j * piece : (j + 1) * piece]) + dot_t(tables[1 + j], last)
            ).astype(BF16)


def experts(received, gate, up, down):
    group = len(received)
    width, hidden = gate.shape
    chunk = 256 if hidden % 256 == 0 else 128
    rows = group * EXPERTS * CAP_DEV
    return pl.pallas_call(
        functools.partial(expert_kernel, chunk, group),
        out_shape=tuple(jax.ShapeDtypeStruct(r.shape, BF16) for r in received),
        in_specs=[VMEM] * (group + 3),
        out_specs=(VMEM,) * group,
        scratch_shapes=[
            pltpu.VMEM((rows, width), BF16),
            pltpu.VMEM((rows, width), F32),
        ],
        compiler_params=pltpu.CompilerParams(vmem_limit_bytes=12 * 1024 * 1024),
        cost_estimate=pl.CostEstimate(
            flops=6 * rows * width * hidden, bytes_accessed=6 * width * hidden, transcendentals=0
        ),
        name="experts",
    )(*received, gate, up, down)


def window(value):
    return pl.pallas_call(
        lambda source, out: None,
        out_shape=jax.ShapeDtypeStruct(value.shape, value.dtype),
        in_specs=[HBM],
        out_specs=HBM,
        input_output_aliases={0: 0},
        compiler_params=pltpu.CompilerParams(vmem_limit_bytes=1024 * 1024),
        cost_estimate=pl.CostEstimate(
            flops=40_000_000_000, bytes_accessed=1024, transcendentals=0
        ),
        name="window",
    )(pin(value))


def combine_kernel(returned, after, combine, out):
    width = after.shape[1]
    piece = width // (SPLIT + 1)

    def blend(table, value):
        high = table.astype(BF16)
        low = (table - high.astype(F32)).astype(BF16)
        return dot_t(high, value) + dot_t(low, value)

    value = returned[...]
    first = blend(combine[0], value)
    last = sum(
        blend(combine[1 + j], value[:, j * piece : (j + 1) * piece]) for j in range(SPLIT)
    )
    at = SPLIT * piece
    out[:, :at] = (after[:, :at] + first).astype(BF16)
    out[:, at:] = (after[:, at:] + last).astype(BF16)


def on_device(
    tokens,
    state,
    norm_gain,
    w_recept,
    w_keys,
    w_values,
    decay_base,
    decay_first_matrix,
    decay_second_matrix,
    rate_base,
    rate_first_matrix,
    rate_second_matrix,
    head_gain,
    w_output,
    second_gain,
    route_ids,
    route_weights,
    expert_gate,
    expert_up,
    expert_down,
):
    devices = lax.axis_size("ep")
    group = devices // EXPERTS
    rows = tokens.shape[0]
    start = (lax.axis_index("ep") * rows).astype(jnp.int32).reshape(1)
    line = lambda a: a.reshape(1, -1)
    packed, after, combine, terms = mixer(
        start,
        (
            tokens,
            line(norm_gain),
            line(decay_base),
            line(rate_base),
            line(head_gain),
            line(second_gain),
            route_ids.T,
            route_weights.T,
        ),
        state,
        (
            w_recept,
            w_keys,
            w_values,
            decay_first_matrix,
            decay_second_matrix,
            rate_first_matrix,
            rate_second_matrix,
            w_output,
        ),
    )
    peers = [[e * group + j for e in range(EXPERTS)] for j in range(group)]
    cols = packed.shape[1]

    def exchange(value):
        chunks = value.reshape(EXPERTS, ROWS, cols)
        out = lax.all_to_all(
            chunks, "ep", split_axis=0, concat_axis=0, tiled=True, axis_index_groups=peers
        )
        return out.reshape(EXPERTS * ROWS, cols)

    def turn(value, by):
        return lax.ppermute(
            value,
            "ep",
            [(i, i // group * group + (i % group + by) % group) for i in range(devices)],
        )

    own = exchange(window(packed))
    new_state = update(state, terms)
    received = (own,) + tuple(turn(own, by) for by in range(1, group))
    results = experts(received, expert_gate, expert_up, expert_down)
    total = results[0].astype(F32)
    for by in range(1, group):
        total = total + turn(results[by], group - by).astype(F32)
    returned = exchange(total.astype(BF16))
    layer_out = pl.pallas_call(
        combine_kernel,
        out_shape=jax.ShapeDtypeStruct(after.shape, BF16),
        in_specs=[VMEM] * 3,
        out_specs=VMEM,
        name="combine",
    )(returned, after, combine)
    return (layer_out, new_state)


def solution(mesh):
    in_specs = (
        P("ep", None),
        P("ep", None, None, None),
        P(),
        P(),
        P(),
        P(),
        P(),
        P(),
        P(),
        P(),
        P(),
        P(),
        P(),
        P(),
        P(),
        P(),
        P(),
        P(None, "ep"),
        P(None, "ep"),
        P("ep", None),
    )
    out_specs = (P("ep", None), P("ep", None, None, None))
    return jax.shard_map(
        on_device, mesh=mesh, in_specs=in_specs, out_specs=out_specs, check_vma=False
    )
```

time: 140 us -> 65.1 us (0.46)
  matrix products: 60.2 us -> 0 us
  Pallas kernels: 0 us -> 31.2 us
  waiting for transfers between devices: 25.4 us -> 6.41 us
  blocking collectives: 33.3 us -> 21.2 us
  other arithmetic: 12.2 us -> 0.84 us
  local copies, waits for them, and re-layouts: 4.1 us -> 0.02 us
    dot_general x12 -> x0, matrix products: 60.2 us -> none  [the longest x1 22 us: time_mixer(): jnp.einsum('bhvk,bhk->bhv', state, unit, precision=lax.Precision.HIGHEST)]
    pallas_call x0 -> x5, Pallas kernels: none -> 31.2 us  [the longest x1 13.7 us: mixer(): pl.pallas_call(mixer_kernel, out_shape=(jax.ShapeDtypeStruct((EXPERTS * R...]
    all_to_all x1, waiting for transfers between devices: 25.4 us -> 3.1 us  [exchange(): lax.all_to_all(chunks, 'ep', split_axis=0, concat_axis=0, tiled=True, axi...]
    all_to_all x1, blocking collectives: 33.3 us -> 21.2 us  [exchange(): lax.all_to_all(chunks, 'ep', split_axis=0, concat_axis=0, tiled=True, axi...]
    add x1 -> x0, other arithmetic: 9.85 us -> none  [time_mixer(): state * d_head[:, :, None, :]]
    ppermute x0 -> x2, waiting for transfers between devices: none -> 3.31 us  [turn(): lax.ppermute(value, 'ep', [(i, i // group * group + (i % group + by) % gr...]
    reduce_sum x6 -> x0, other arithmetic: 1.83 us -> none  [the longest x1 1.12 us: norm_rows(): mean_sq = jnp.mean(values * values, axis=-1, keepdims=True)]
    dynamic_slice x2 -> x0, local copies, waits for them, and re-layouts: 1.52 us -> none  [the longest x1 0.76 us: on_device(): own_weights = lax.dynamic_slice_in_dim(route_weights, start, rows_dev, 0)]
  transfers between devices with their start and end apart: 1 -> 3, of which waited for: 1 -> 3; matrix products, arithmetic and copies ran while one was open for 1% -> 0% of each run, Pallas kernels for 0% -> 16%
where the time goes in v1:
time: 65.1 us; the launch traced here: 64.8 us
  Pallas kernels  31.2 us (48%)
  blocking collectives  21.2 us (33%)
  waiting for transfers between devices  6.41 us (10%)
  starting transfers between devices  4.4 us (7%)
  other arithmetic  0.84 us (1%)
  between operations  0.71 us (1%)
    all_to_all x1, blocking collectives, exchange(): lax.all_to_all(chunks, 'ep', split_axis=0, concat_axis=0, tiled=True, axi...  21.2 us
    pallas_call x1, Pallas kernels, mixer(): pl.pallas_call(mixer_kernel, out_shape=(jax.ShapeDtypeStruct((EXPERTS * R...  13.7 us
    pallas_call x1, Pallas kernels, update(): pl.pallas_call(update_kernel, out_shape=jax.ShapeDtypeStruct(state.shape,...  10.1 us
    pallas_call x1, Pallas kernels, experts(): pl.pallas_call(functools.partial(expert_kernel, chunk, group), out_shape=...  5.28 us
    all_to_all x1, starting transfers between devices, exchange(): lax.all_to_all(chunks, 'ep', split_axis=0, concat_axis=0, tiled=True, axi...  4.2 us
    ppermute x2, waiting for transfers between devices, turn(): lax.ppermute(value, 'ep', [(i, i // group * group + (i % group + by) % gr...  3.31 us
    all_to_all x1, waiting for transfers between devices, exchange(): lax.all_to_all(chunks, 'ep', split_axis=0, concat_axis=0, tiled=True, axi...  3.1 us
    pallas_call x1, Pallas kernels, on_device(): pl.pallas_call(combine_kernel, out_shape=jax.ShapeDtypeStruct(after.shape...  2.2 us
  transfers between devices with their start and end apart: 3, of which 3 were waited for; matrix products, arithmetic and copies ran while one was open for 0% of the time, Pallas kernels for 16%

profile of v1, /device:TPU:0, one launch (start us, length us, event | category | flops | bytes accessed | tf_op | source)
XLA Modules:
  0.0 64.8 jit_solution(9886693524960756533)
XLA Ops:
  0.6 13.7 %mixer.1 = (bf16[128,1536]{1,0:T(8,128)(2,1)}, f32[24,2048]{1,0:T(8,128)}, f32[4,128,24]{2,1,0:T(8,128)}, f32[5,24,1024]{2,1,0:T(8,128)}) custom-call(s32[1]{0:T(128)} %bitcast.start, bf16[24,2048]{1,0:T(8,128)(2,1)} %tokens_in.1, f32[1,2048]{1,0:T(1,128)} %bitcast.16, f32[1,1024]{1,0:T(1,128)} %bitcast.20, f32[1,1024]{1,0:T(1,128)} %bitcast.21, ...), custom_call_target="tpu_custom_call" | custom-call | flops 24000000000 | bytes 30000000 | tf_op jit(solution)/shard_map/mixer/pallas_call | solution.py:278
  14.3 0.0 copy-start
  14.3 0.0 copy-start.1
  14.3 0.0 copy-start.2
  14.4 21.2 %all_to_all.10 = bf16[16,8,1536]{2,1,0:T(8,128)(2,1)S(1)} all-to-all(bf16[16,8,1536]{2,1,0:T(8,128)(2,1)} %bitcast.15), channel_id=1, replica_groups={{0,2,4,6,8,10,12,14,16,18,20,22,24,26,28,30},{1,3,5,7,9,11,13,15,17,19,..., dimensions={0} | all-to-all | bytes 786432 | tf_op jit(solution)/shard_map/all_to_all | solution.py:551
  35.6 0.0 collective-permute-start
  35.6 1.7 %collective-permute-done.refs_1_ = bf16[128,1536]{1,0:T(8,128)(2,1)S(1)} collective-permute-done((bf16[128,1536]{1,0:T(8,128)(2,1)S(1)}, bf16[128,1536]{1,0:T(8,128)(2,1)S(1)}, u32[]{:S(2)}, u32[]{:S(2)}) %collective-permute-start) | collective-permute-done | bytes 393248 | tf_op jit(solution)/shard_map/ppermute | solution.py:557
  37.3 0.0 copy-done
  37.3 0.0 copy-done.1
  37.3 0.0 copy-done.2
  37.3 5.3 %experts.1 = (bf16[128,1536]{1,0:T(8,128)(2,1)S(1)}, bf16[128,1536]{1,0:T(8,128)(2,1)S(1)}) custom-call(bf16[128,1536]{1,0:T(8,128)(2,1)S(1)} %bitcast.14, bf16[128,1536]{1,0:T(8,128)(2,1)S(1)} %collective-permute-done.refs_1_, bf16[2048,1536]{1,0:T(8,128)(2,1)S(1)} %copy-done, bf16[2048,1536]{1,0:T(8,128)(2,1)S(1)} %copy-done.1, ...), custom_call_target="tpu_custom_call" | custom-call | flops 3623878656 | bytes 18874368 | tf_op jit(solution)/shard_map/experts/pallas_call | solution.py:444
  42.6 0.2 collective-permute-start.1
  42.8 1.6 %collective-permute-done.1 = bf16[128,1536]{1,0:T(8,128)(2,1)S(1)} collective-permute-done((bf16[128,1536]{1,0:T(8,128)(2,1)S(1)}, bf16[128,1536]{1,0:T(8,128)(2,1)S(1)}, u32[]{:S(2)}, u32[]{:S(2)}) %collective-permute-start.1) | collective-permute-done | bytes 393248 | tf_op jit(solution)/shard_map/ppermute | solution.py:557
  44.4 0.8 %fusion = bf16[16,8,1536]{2,1,0:T(8,128)(2,1)} fusion(bf16[128,1536]{1,0:T(8,128)(2,1)S(1)} %collective-permute-done.1, bf16[128,1536]{1,0:T(8,128)(2,1)S(1)} %get-tuple-element.9), kind=kLoop, calls=%fused_computation.1 | loop fusion | flops 786432 | bytes 1179648 | tf_op jit(solution)/shard_map/reshape | solution.py:550
  45.3 4.2 %all-to-all-start.1 = ((bf16[16,8,1536]{2,1,0:T(8,128)(2,1)}), bf16[16,8,1536]{2,1,0:T(8,128)(2,1)}, u32[]{:S(2)}, u32[]{:S(2)}) async-start(bf16[16,8,1536]{2,1,0:T(8,128)(2,1)} %fusion), calls=%async_computation.1 | async-start | bytes 786432 | tf_op jit(solution)/shard_map/all_to_all | solution.py:551
  49.5 10.1 %update.1 = f32[24,16,64,64]{3,2,1,0:T(8,128)} custom-call(f32[24,16,64,64]{3,2,1,0:T(8,128)} %state.3, f32[5,24,1024]{2,1,0:T(8,128)} %get-tuple-element.13.terms_in), custom_call_target="tpu_custom_call" | custom-call | flops 16000000000 | bytes 26000000 | tf_op jit(solution)/shard_map/update/pallas_call | solution.py:375
  59.5 3.1 %all-to-all-done.1 = bf16[16,8,1536]{2,1,0:T(8,128)(2,1)} async-done(((bf16[16,8,1536]{2,1,0:T(8,128)(2,1)}), bf16[16,8,1536]{2,1,0:T(8,128)(2,1)}, u32[]{:S(2)}, u32[]{:S(2)}) %all-to-all-start.1) | async-done | bytes 393248 | tf_op jit(solution)/shard_map/all_to_all | solution.py:551
  62.6 2.2 %combine.1 = bf16[24,2048]{1,0:T(8,128)(2,1)} custom-call(bf16[128,1536]{1,0:T(8,128)(2,1)} %bitcast.11.returned, f32[24,2048]{1,0:T(8,128)} %get-tuple-element.11.after, f32[4,128,24]{2,1,0:T(8,128)} %get-tuple-element.12.combine), custom_call_target="tpu_custom_call" | custom-call | tf_op jit(solution)/shard_map/combine/pallas_call | solution.py:571
  (1 shorter events, 0.0 us)
Async XLA Ops:
  14.3 23.0 %copy-start = (bf16[2048,1536]{1,0:T(8,128)(2,1)S(1)}, bf16[2048,1536]{1,0:T(8,128)(2,1)}, u32[]{:S(2)}) copy-start(bf16[2048,1536]{1,0:T(8,128)(2,1)} %refs_2_.1) | copy-start | bytes 18874372
  14.3 23.0 %copy-start.1 = (bf16[2048,1536]{1,0:T(8,128)(2,1)S(1)}, bf16[2048,1536]{1,0:T(8,128)(2,1)}, u32[]{:S(2)}) copy-start(bf16[2048,1536]{1,0:T(8,128)(2,1)} %refs_3_.1) | copy-start | bytes 18874372
  14.3 23.0 %copy-start.2 = (bf16[1536,2048]{1,0:T(8,128)(2,1)S(1)}, bf16[1536,2048]{1,0:T(8,128)(2,1)}, u32[]{:S(2)}) copy-start(bf16[1536,2048]{1,0:T(8,128)(2,1)} %refs_4_.1) | copy-start | bytes 18874372
  35.6 1.7 %collective-permute-start = (bf16[128,1536]{1,0:T(8,128)(2,1)S(1)}, bf16[128,1536]{1,0:T(8,128)(2,1)S(1)}, u32[]{:S(2)}, u32[]{:S(2)}) collective-permute-start(bf16[128,1536]{1,0:T(8,128)(2,1)S(1)} %bitcast.13), channel_id=1, source_target_pairs={{0,1},{1,0},{2,3},{3,2},{4,5},{5,4},{6,7},{7,6},{8,9},{9,8},{10,11... | collective-permute-start | bytes 1179656 | tf_op jit(solution)/shard_map/ppermute | solution.py:557
  42.6 1.8 %collective-permute-start.1 = (bf16[128,1536]{1,0:T(8,128)(2,1)S(1)}, bf16[128,1536]{1,0:T(8,128)(2,1)S(1)}, u32[]{:S(2)}, u32[]{:S(2)}) collective-permute-start(bf16[128,1536]{1,0:T(8,128)(2,1)S(1)} %get-tuple-element.10), channel_id=1, source_target_pairs={{0,1},{1,0},{2,3},{3,2},{4,5},{5,4},{6,7},{7,6},{8,9},{9,8},{10,11... | collective-permute-start | bytes 1179656 | tf_op jit(solution)/shard_map/ppermute | solution.py:557
  45.3 17.4 %all-to-all-start.1 = ((bf16[16,8,1536]{2,1,0:T(8,128)(2,1)}), bf16[16,8,1536]{2,1,0:T(8,128)(2,1)}, u32[]{:S(2)}, u32[]{:S(2)}) async-start(bf16[16,8,1536]{2,1,0:T(8,128)(2,1)} %fusion), calls=%async_computation.1 | async-start | bytes 786432 | tf_op jit(solution)/shard_map/all_to_all | solution.py:551

commit v2 on v1

--- a/solution.py
+++ b/solution.py
@@ -61,10 +61,12 @@
     rate_first,
     rate_second,
     w_output,
-    packed,
-    after_out,
+    packed_out,
+    after,
     combine,
     terms_out,
+    packed,
+    terms,
     s_buf,
     wr_buf,
     wk_buf,
@@ -87,8 +89,9 @@
     w_sem,
     s_sem,
     a_sem,
+    o_sem,
 ):
-    keys_out, vals_out, decay_out, ua_out, probe_out = (terms_out.at[i] for i in range(5))
+    keys_out, vals_out, decay_out, ua_out, probe_out = (terms.at[i] for i in range(5))
     rows, width = tokens.shape
     small = [
         pltpu.make_async_copy(src, dst, a_sem.at[i])
@@ -133,12 +136,33 @@
         weight(7 + i, w_output.at[pl.ds(i * half, half)], wo_buf.at[pl.ds(i * half, half)])
         for i in range(2)
     ]
-    for copy in (k_copy, d1_copy, r1_copy, d2_copy, r2_copy, r_copy):
-        copy.start()
-
+    k_copy.start()
     for copy in small:
         copy.wait()
 
+    resid = tokens[...].astype(F32)
+    mean_sq = jnp.mean(resid * resid, axis=1, keepdims=True)
+    normed = (resid * lax.rsqrt(mean_sq + 1e-06) * norm_gain[...]).astype(BF16)
+
+    for copy in (d1_copy, r1_copy, d2_copy, r2_copy, r_copy):
+        copy.start()
+    k_copy.wait()
+    v_copy.start()
+    keys_out[...] = dot(normed, wk_buf[...]).astype(BF16).astype(F32)
+    for copy in (d1_copy, r1_copy, d2_copy, r2_copy):
+        copy.wait()
+    decay_low = jnp.tanh(dot(normed, d1_buf[...])).astype(BF16)
+    rate_low = dot(normed, r1_buf[...]).astype(BF16)
+    pre = decay_base[...] + dot(decay_low, d2_buf[...])
+    decay_out[...] = jnp.exp(-jnp.exp(-jax.nn.softplus(-pre) - 0.5))
+    rate = jax.nn.sigmoid(rate_base[...] + dot(rate_low, r2_buf[...]))
+    state_copy(0).start()
+    r_copy.wait()
+    state_copy(1).start()
+    recept = dot(normed, wr_buf[...]).astype(BF16).astype(F32)
+    v_copy.wait()
+    for g in range(2, groups):
+        state_copy(g).start()
     all_rows = ids_t.shape[1]
     pick = (iota((all_rows, rows), 0) == iota((all_rows, rows), 1) + start[0]).astype(F32)
     own_ids = jnp.dot(ids_t[...].astype(F32), pick, preferred_element_type=F32)
@@ -163,30 +187,9 @@
         slot = SPLIT * (row - CAP_DEV) + j
         tables.append(jnp.where(member_r & (row >= CAP_DEV) & (order_r == slot), 1.0, 0.0))
     for j in range(SPLIT + 1):
-        combine[j] = tables[j] * share_r
-
-    resid = tokens[...].astype(F32)
-    mean_sq = jnp.mean(resid * resid, axis=1, keepdims=True)
-    normed = (resid * lax.rsqrt(mean_sq + 1e-06) * norm_gain[...]).astype(BF16)
-
-    k_copy.wait()
-    state_copy(0).start()
-    keys_out[...] = dot(normed, wk_buf[...]).astype(BF16).astype(F32)
-    d1_copy.wait()
-    decay_low = jnp.tanh(dot(normed, d1_buf[...])).astype(BF16)
-    r1_copy.wait()
-    state_copy(1).start()
-    rate_low = dot(normed, r1_buf[...]).astype(BF16)
-    d2_copy.wait()
-    pre = decay_base[...] + dot(decay_low, d2_buf[...])
-    decay_out[...] = jnp.exp(-jnp.exp(-jax.nn.softplus(-pre) - 0.5))
-    r2_copy.wait()
-    rate = jax.nn.sigmoid(rate_base[...] + dot(rate_low, r2_buf[...]))
-    r_copy.wait()
-    for g in range(2, groups):
-        state_copy(g).start()
-    v_copy.start()
-    recept = dot(normed, wr_buf[...]).astype(BF16).astype(F32)
+        combine[j] = (tables[j] * share_r).T
+
+    vals_out[...] = dot(normed, wv_buf[...]).astype(BF16).astype(F32)
 
     for p in range(pairs):
         at = slice(p * 128, p * 128 + 128)
@@ -213,18 +216,11 @@
             total = total + jnp.where(own_block & (token == c), x[:, c * 128 : c * 128 + 128], 0.0)
         return total + pltpu.roll(total, 64, 1)
 
-    def state_step(g, carry):
-        state_copy(g).wait()
-
-        @pl.when(g == 1)
-        def _():
-            for copy in o_copies:
-                copy.start()
-
-        for p in range(step // 2):
+    def read_out(g):
+        for p in range(g * step // 2, (g + 1) * step // 2):
+            at = slice(p * 128, p * 128 + 128)
             found = []
-            for h in range(2):
-                head = g * step + 2 * p + h
+            for head in (2 * p, 2 * p + 1):
                 block = s_buf[:, head].reshape(rows * 64, 64).astype(BF16)
                 found.append(
                     lax.dot_general(
@@ -234,37 +230,54 @@
                         preferred_element_type=F32,
                     )
                 )
-            at = pl.ds(pl.multiple_of((g * step + 2 * p) * 64, 128), 128)
             probe_out[:, at] = jnp.where(low, diagonal(found[0][:rows]), diagonal(found[1][:rows]))
             sums[2, :, at] = jnp.where(low, diagonal(found[0][rows:]), diagonal(found[1][rows:]))
-        return carry
-
-    lax.fori_loop(0, groups, state_step, 0)
-
-    v_copy.wait()
-    vals_out[...] = dot(normed, wv_buf[...]).astype(BF16).astype(F32)
-    pieces = []
-    for p in range(pairs):
+
+    def normalized(p):
         at = slice(p * 128, p * 128 + 128)
-        mixed = sums[2, :, at] - probe_out[:, at] * sums[0, :, at] + vals_out[:, at] * sums[1, :, at]
+        mixed = sums[2, :, at] - probe_out[:, at] * sums[0, :, at]
+        mixed = mixed + vals_out[:, at] * sums[1, :, at]
         centre = mixed - head_sums(mixed) * (1.0 / 64)
         var = head_sums(centre * centre) * (1.0 / 64)
-        pieces.append((centre * lax.rsqrt(var + 0.00064) * head_gain[:, at]).astype(BF16))
+        return (centre * lax.rsqrt(var + 0.00064) * head_gain[:, at]).astype(BF16)
+
+    pieces = []
+    for g in range(groups):
+        state_copy(g).wait()
+        if g == 0:
+            for copy in o_copies:
+                copy.start()
+        read_out(g)
+        if g:
+            pieces += [normalized(p) for p in range((g - 1) * step // 2, g * step // 2)]
+    pieces += [normalized(p) for p in range((groups - 1) * step // 2, pairs)]
     mixed = jnp.concatenate(pieces, axis=1)
-    after = resid
+    total = resid
     for i in range(2):
         o_copies[i].wait()
-        after = after + dot(mixed[:, i * half : i * half + half], wo_buf[pl.ds(i * half, half)])
-    after_out[...] = after
-    mean_sq = jnp.mean(after * after, axis=1, keepdims=True)
-    second = (after * lax.rsqrt(mean_sq + 1e-06) * second_gain[...]).astype(BF16)
+        total = total + dot(mixed[:, i * half : i * half + half], wo_buf[pl.ds(i * half, half)])
+    after[...] = total
+    terms_copy = pltpu.make_async_copy(terms, terms_out, o_sem.at[0])
+    terms_copy.start()
+
+    mean_sq = jnp.mean(total * total, axis=1, keepdims=True)
+    second = (total * lax.rsqrt(mean_sq + 1e-06) * second_gain[...]).astype(BF16)
     piece = width // (SPLIT + 1)
     last = second[:, SPLIT * piece :]
+    copies = []
     for j in range(SPLIT):
-        packed[:, j * piece : (j + 1) * piece] = (
-            dot(tables[0].astype(BF16), second[:, j * piece : (j + 1) * piece])
-            + dot(tables[1 + j].astype(BF16), last)
+        at = slice(j * piece, (j + 1) * piece)
+        packed[:, at] = (
+            dot(tables[0].astype(BF16), second[:, at]) + dot(tables[1 + j].astype(BF16), last)
         ).astype(BF16)
+        at = pl.ds(j * piece, piece)
+        copies.append(
+            pltpu.make_async_copy(packed.at[:, at], packed_out.at[:, at], o_sem.at[1 + j])
+        )
+        copies[j].start()
+    terms_copy.wait()
+    for copy in copies:
+        copy.wait()
 
 
 def mixer(start, args, state, mats):
@@ -278,14 +291,16 @@
     return pl.pallas_call(
         mixer_kernel,
         out_shape=(
-            jax.ShapeDtypeStruct((EXPERTS * ROWS, width * SPLIT // (SPLIT + 1)), BF16),
+            pltpu.HBM((EXPERTS * ROWS, width * SPLIT // (SPLIT + 1)), BF16),
             f(rows, width),
-            f(SPLIT + 1, EXPERTS * ROWS, rows),
-            f(5, rows, chan),
+            f(SPLIT + 1, rows, EXPERTS * ROWS),
+            pltpu.HBM((5, rows, chan), F32),
         ),
         in_specs=[SMEM] + [HBM] * (len(args) + 1 + len(mats)),
-        out_specs=(VMEM,) * 4,
+        out_specs=(HBM, VMEM, VMEM, HBM),
         scratch_shapes=[
+            v((EXPERTS * ROWS, width * SPLIT // (SPLIT + 1)), BF16),
+            v((5, rows, chan), F32),
             v(state.shape, F32),
             v((width, chan), BF16),
             v((width, chan), BF16),
@@ -301,6 +316,7 @@
             pltpu.SemaphoreType.DMA((9,)),
             pltpu.SemaphoreType.DMA((groups,)),
             pltpu.SemaphoreType.DMA((len(args),)),
+            pltpu.SemaphoreType.DMA((1 + SPLIT,)),
         ],
         compiler_params=pltpu.CompilerParams(vmem_limit_bytes=67_000_000),
         cost_estimate=pl.CostEstimate(
@@ -385,7 +401,7 @@
             pltpu.VMEM(terms.shape, F32),
             pltpu.SemaphoreType.DMA((1,)),
         ],
-        compiler_params=pltpu.CompilerParams(vmem_limit_bytes=67_000_000),
+        compiler_params=pltpu.CompilerParams(vmem_limit_bytes=32 * 1024 * 1024),
         cost_estimate=pl.CostEstimate(
             flops=16_000_000_000, bytes_accessed=26_000_000, transcendentals=0
         ),
@@ -480,7 +496,7 @@
     def blend(table, value):
         high = table.astype(BF16)
         low = (table - high.astype(F32)).astype(BF16)
-        return dot_t(high, value) + dot_t(low, value)
+        return dot(high, value) + dot(low, value)
 
     value = returned[...]
     first = blend(combine[0], value)
@@ -573,6 +589,7 @@
         out_shape=jax.ShapeDtypeStruct(after.shape, BF16),
         in_specs=[VMEM] * 3,
         out_specs=VMEM,
+        compiler_params=pltpu.CompilerParams(vmem_limit_bytes=8 * 1024 * 1024),
         name="combine",
     )(returned, after, combine)
     return (layer_out, new_state)

time: 65.1 us -> 63 us (0.968)
  Pallas kernels: 31.2 us -> 29.9 us
    pallas_call x1, Pallas kernels: 2.2 us -> 0.99 us  [on_device(): pl.pallas_call(combine_kernel, out_shape=jax.ShapeDtypeStruct(after.shape...]
where the time goes in v2:
time: 63 us; the launch traced here: 62.7 us
  Pallas kernels  29.9 us (47%)
  blocking collectives  21.2 us (34%)
  waiting for transfers between devices  6.27 us (10%)
  starting transfers between devices  3.78 us (6%)
  other arithmetic  0.84 us (1%)
  between operations  0.73 us (1%)
    all_to_all x1, blocking collectives, exchange(): lax.all_to_all(chunks, 'ep', split_axis=0, concat_axis=0, tiled=True, axi...  21.2 us
    pallas_call x1, Pallas kernels, mixer(): pl.pallas_call(mixer_kernel, out_shape=(pltpu.HBM((EXPERTS * ROWS, width...  13.5 us
    pallas_call x1, Pallas kernels, update(): pl.pallas_call(update_kernel, out_shape=jax.ShapeDtypeStruct(state.shape,...  10.1 us
    pallas_call x1, Pallas kernels, experts(): pl.pallas_call(functools.partial(expert_kernel, chunk, group), out_shape=...  5.29 us
    all_to_all x1, starting transfers between devices, exchange(): lax.all_to_all(chunks, 'ep', split_axis=0, concat_axis=0, tiled=True, axi...  3.6 us
    ppermute x2, waiting for transfers between devices, turn(): lax.ppermute(value, 'ep', [(i, i // group * group + (i % group + by) % gr...  3.32 us
    all_to_all x1, waiting for transfers between devices, exchange(): lax.all_to_all(chunks, 'ep', split_axis=0, concat_axis=0, tiled=True, axi...  2.94 us
  transfers between devices with their start and end apart: 3, of which 3 were waited for; matrix products, arithmetic and copies ran while one was open for 0% of the time, Pallas kernels for 16%

profile of v2, /device:TPU:0, one launch (start us, length us, event | category | flops | bytes accessed | tf_op | source)
XLA Modules:
  0.0 62.7 jit_solution(15525676548659714459)
XLA Ops:
  0.6 13.5 %mixer.1 = (bf16[128,1536]{1,0:T(8,128)(2,1)}, f32[24,2048]{1,0:T(8,128)}, f32[4,24,128]{2,1,0:T(8,128)}, f32[5,24,1024]{2,1,0:T(8,128)}) custom-call(s32[1]{0:T(128)} %bitcast.start, bf16[24,2048]{1,0:T(8,128)(2,1)} %tokens_in.1, f32[1,2048]{1,0:T(1,128)} %bitcast.17, f32[1,1024]{1,0:T(1,128)} %bitcast.21, f32[1,1024]{1,0:T(1,128)} %bitcast.22, ...), custom_call_target="tpu_custom_call" | custom-call | flops 24000000000 | bytes 30000000 | tf_op jit(solution)/shard_map/mixer/pallas_call | solution.py:291
  14.1 0.0 copy-start
  14.1 0.0 copy-start.1
  14.2 0.0 copy-start.2
  14.2 21.2 %all_to_all.10 = bf16[16,8,1536]{2,1,0:T(8,128)(2,1)S(1)} all-to-all(bf16[16,8,1536]{2,1,0:T(8,128)(2,1)} %bitcast.16), channel_id=1, replica_groups={{0,2,4,6,8,10,12,14,16,18,20,22,24,26,28,30},{1,3,5,7,9,11,13,15,17,19,..., dimensions={0} | all-to-all | bytes 786432 | tf_op jit(solution)/shard_map/all_to_all | solution.py:567
  35.4 0.0 collective-permute-start
  35.4 1.7 %collective-permute-done.refs_1_ = bf16[128,1536]{1,0:T(8,128)(2,1)S(1)} collective-permute-done((bf16[128,1536]{1,0:T(8,128)(2,1)S(1)}, bf16[128,1536]{1,0:T(8,128)(2,1)S(1)}, u32[]{:S(2)}, u32[]{:S(2)}) %collective-permute-start) | collective-permute-done | bytes 393248 | tf_op jit(solution)/shard_map/ppermute | solution.py:573
  37.1 0.0 copy-done
  37.1 0.0 copy-done.1
  37.1 0.0 copy-done.2
  37.1 5.3 %experts.1 = (bf16[128,1536]{1,0:T(8,128)(2,1)S(1)}, bf16[128,1536]{1,0:T(8,128)(2,1)S(1)}) custom-call(bf16[128,1536]{1,0:T(8,128)(2,1)S(1)} %bitcast.15, bf16[128,1536]{1,0:T(8,128)(2,1)S(1)} %collective-permute-done.refs_1_, bf16[2048,1536]{1,0:T(8,128)(2,1)S(1)} %copy-done, bf16[2048,1536]{1,0:T(8,128)(2,1)S(1)} %copy-done.1, ...), custom_call_target="tpu_custom_call" | custom-call | flops 3623878656 | bytes 18874368 | tf_op jit(solution)/shard_map/experts/pallas_call | solution.py:460
  42.4 0.2 collective-permute-start.1
  42.6 1.6 %collective-permute-done.1 = bf16[128,1536]{1,0:T(8,128)(2,1)S(1)} collective-permute-done((bf16[128,1536]{1,0:T(8,128)(2,1)S(1)}, bf16[128,1536]{1,0:T(8,128)(2,1)S(1)}, u32[]{:S(2)}, u32[]{:S(2)}) %collective-permute-start.1) | collective-permute-done | bytes 393248 | tf_op jit(solution)/shard_map/ppermute | solution.py:573
  44.2 0.8 %fusion = bf16[16,8,1536]{2,1,0:T(8,128)(2,1)} fusion(bf16[128,1536]{1,0:T(8,128)(2,1)S(1)} %collective-permute-done.1, bf16[128,1536]{1,0:T(8,128)(2,1)S(1)} %get-tuple-element.9), kind=kLoop, calls=%fused_computation.1 | loop fusion | flops 786432 | bytes 1179648 | tf_op jit(solution)/shard_map/reshape | solution.py:566
  45.1 3.6 %all-to-all-start.1 = ((bf16[16,8,1536]{2,1,0:T(8,128)(2,1)}), bf16[16,8,1536]{2,1,0:T(8,128)(2,1)S(1)}, u32[]{:S(2)}, u32[]{:S(2)}) async-start(bf16[16,8,1536]{2,1,0:T(8,128)(2,1)} %fusion), calls=%async_computation.1 | async-start | bytes 786432 | tf_op jit(solution)/shard_map/all_to_all | solution.py:567
  48.7 0.0 copy-start.3
  48.7 0.0 copy-start.4
  48.7 10.1 %update.1 = f32[24,16,64,64]{3,2,1,0:T(8,128)} custom-call(f32[24,16,64,64]{3,2,1,0:T(8,128)} %state.3, f32[5,24,1024]{2,1,0:T(8,128)} %get-tuple-element.13.terms_in), custom_call_target="tpu_custom_call" | custom-call | flops 16000000000 | bytes 26000000 | tf_op jit(solution)/shard_map/update/pallas_call | solution.py:391
  58.8 2.9 %all-to-all-done.1 = bf16[16,8,1536]{2,1,0:T(8,128)(2,1)S(1)} async-done(((bf16[16,8,1536]{2,1,0:T(8,128)(2,1)}), bf16[16,8,1536]{2,1,0:T(8,128)(2,1)S(1)}, u32[]{:S(2)}, u32[]{:S(2)}) %all-to-all-start.1) | async-done | bytes 393248 | tf_op jit(solution)/shard_map/all_to_all | solution.py:567
  61.7 0.0 copy-done.3
  61.8 0.0 copy-done.4
  61.8 1.0 %combine.1 = bf16[24,2048]{1,0:T(8,128)(2,1)} custom-call(bf16[128,1536]{1,0:T(8,128)(2,1)S(1)} %bitcast.13, f32[24,2048]{1,0:T(8,128)S(1)} %copy-done.3, f32[4,24,128]{2,1,0:T(8,128)S(1)} %copy-done.4), custom_call_target="tpu_custom_call" | custom-call | tf_op jit(solution)/shard_map/combine/pallas_call | solution.py:587
  (1 shorter events, 0.0 us)
Async XLA Ops:
  14.1 23.0 %copy-start = (bf16[2048,1536]{1,0:T(8,128)(2,1)S(1)}, bf16[2048,1536]{1,0:T(8,128)(2,1)}, u32[]{:S(2)}) copy-start(bf16[2048,1536]{1,0:T(8,128)(2,1)} %refs_2_.1) | copy-start | bytes 18874372
  14.1 23.0 %copy-start.1 = (bf16[2048,1536]{1,0:T(8,128)(2,1)S(1)}, bf16[2048,1536]{1,0:T(8,128)(2,1)}, u32[]{:S(2)}) copy-start(bf16[2048,1536]{1,0:T(8,128)(2,1)} %refs_3_.1) | copy-start | bytes 18874372
  14.2 23.0 %copy-start.2 = (bf16[1536,2048]{1,0:T(8,128)(2,1)S(1)}, bf16[1536,2048]{1,0:T(8,128)(2,1)}, u32[]{:S(2)}) copy-start(bf16[1536,2048]{1,0:T(8,128)(2,1)} %refs_4_.1) | copy-start | bytes 18874372
  35.4 1.7 %collective-permute-start = (bf16[128,1536]{1,0:T(8,128)(2,1)S(1)}, bf16[128,1536]{1,0:T(8,128)(2,1)S(1)}, u32[]{:S(2)}, u32[]{:S(2)}) collective-permute-start(bf16[128,1536]{1,0:T(8,128)(2,1)S(1)} %bitcast.14), channel_id=1, source_target_pairs={{0,1},{1,0},{2,3},{3,2},{4,5},{5,4},{6,7},{7,6},{8,9},{9,8},{10,11... | collective-permute-start | bytes 1179656 | tf_op jit(solution)/shard_map/ppermute | solution.py:573
  42.4 1.8 %collective-permute-start.1 = (bf16[128,1536]{1,0:T(8,128)(2,1)S(1)}, bf16[128,1536]{1,0:T(8,128)(2,1)S(1)}, u32[]{:S(2)}, u32[]{:S(2)}) collective-permute-start(bf16[128,1536]{1,0:T(8,128)(2,1)S(1)} %get-tuple-element.10), channel_id=1, source_target_pairs={{0,1},{1,0},{2,3},{3,2},{4,5},{5,4},{6,7},{7,6},{8,9},{9,8},{10,11... | collective-permute-start | bytes 1179656 | tf_op jit(solution)/shard_map/ppermute | solution.py:573
  45.1 16.7 %all-to-all-start.1 = ((bf16[16,8,1536]{2,1,0:T(8,128)(2,1)}), bf16[16,8,1536]{2,1,0:T(8,128)(2,1)S(1)}, u32[]{:S(2)}, u32[]{:S(2)}) async-start(bf16[16,8,1536]{2,1,0:T(8,128)(2,1)} %fusion), calls=%async_computation.1 | async-start | bytes 786432 | tf_op jit(solution)/shard_map/all_to_all | solution.py:567
  48.7 13.1 %copy-start.3 = (f32[24,2048]{1,0:T(8,128)S(1)}, f32[24,2048]{1,0:T(8,128)}, u32[]{:S(2)}) copy-start(f32[24,2048]{1,0:T(8,128)} %get-tuple-element.11.after) | copy-start | bytes 589828
  48.7 13.1 %copy-start.4 = (f32[4,24,128]{2,1,0:T(8,128)S(1)}, f32[4,24,128]{2,1,0:T(8,128)}, u32[]{:S(2)}) copy-start(f32[4,24,128]{2,1,0:T(8,128)} %get-tuple-element.12.combine) | copy-start | bytes 147460

commit v3 on v2

--- a/solution.py
+++ b/solution.py
@@ -136,7 +136,8 @@
         weight(7 + i, w_output.at[pl.ds(i * half, half)], wo_buf.at[pl.ds(i * half, half)])
         for i in range(2)
     ]
-    k_copy.start()
+    for copy in (d1_copy, r1_copy, d2_copy, r2_copy, k_copy):
+        copy.start()
     for copy in small:
         copy.wait()
 
@@ -144,20 +145,19 @@
     mean_sq = jnp.mean(resid * resid, axis=1, keepdims=True)
     normed = (resid * lax.rsqrt(mean_sq + 1e-06) * norm_gain[...]).astype(BF16)
 
-    for copy in (d1_copy, r1_copy, d2_copy, r2_copy, r_copy):
-        copy.start()
-    k_copy.wait()
-    v_copy.start()
-    keys_out[...] = dot(normed, wk_buf[...]).astype(BF16).astype(F32)
     for copy in (d1_copy, r1_copy, d2_copy, r2_copy):
         copy.wait()
+    r_copy.start()
     decay_low = jnp.tanh(dot(normed, d1_buf[...])).astype(BF16)
     rate_low = dot(normed, r1_buf[...]).astype(BF16)
     pre = decay_base[...] + dot(decay_low, d2_buf[...])
     decay_out[...] = jnp.exp(-jnp.exp(-jax.nn.softplus(-pre) - 0.5))
     rate = jax.nn.sigmoid(rate_base[...] + dot(rate_low, r2_buf[...]))
+    k_copy.wait()
+    v_copy.start()
+    keys_out[...] = dot(normed, wk_buf[...]).astype(BF16).astype(F32)
+    r_copy.wait()
     state_copy(0).start()
-    r_copy.wait()
     state_copy(1).start()
     recept = dot(normed, wr_buf[...]).astype(BF16).astype(F32)
     v_copy.wait()
@@ -455,7 +455,7 @@
 def experts(received, gate, up, down):
     group = len(received)
     width, hidden = gate.shape
-    chunk = 256 if hidden % 256 == 0 else 128
+    chunk = next(c for c in (768, 384, 128) if hidden % c == 0)
     rows = group * EXPERTS * CAP_DEV
     return pl.pallas_call(
         functools.partial(expert_kernel, chunk, group),
@@ -466,7 +466,7 @@
             pltpu.VMEM((rows, width), BF16),
             pltpu.VMEM((rows, width), F32),
         ],
-        compiler_params=pltpu.CompilerParams(vmem_limit_bytes=12 * 1024 * 1024),
+        compiler_params=pltpu.CompilerParams(vmem_limit_bytes=16 * 1024 * 1024),
         cost_estimate=pl.CostEstimate(
             flops=6 * rows * width * hidden, bytes_accessed=6 * width * hidden, transcendentals=0
         ),

time: 63 us -> 61.7 us (0.979)
  Pallas kernels: 29.9 us -> 28.6 us
    pallas_call x1, Pallas kernels: 13.5 us -> 12.8 us  [mixer(): pl.pallas_call(mixer_kernel, out_shape=(pltpu.HBM((EXPERTS * ROWS, width...]
where the time goes in v3:
time: 61.7 us; the launch traced here: 61.5 us
  Pallas kernels  28.6 us (46%)
  blocking collectives  21.2 us (34%)
  waiting for transfers between devices  6.25 us (10%)
  starting transfers between devices  3.8 us (6%)
  other arithmetic  0.84 us (1%)
  between operations  0.73 us (1%)
    all_to_all x1, blocking collectives, exchange(): lax.all_to_all(chunks, 'ep', split_axis=0, concat_axis=0, tiled=True, axi...  21.2 us
    pallas_call x1, Pallas kernels, mixer(): pl.pallas_call(mixer_kernel, out_shape=(pltpu.HBM((EXPERTS * ROWS, width...  12.8 us
    pallas_call x1, Pallas kernels, update(): pl.pallas_call(update_kernel, out_shape=jax.ShapeDtypeStruct(state.shape,...  10.1 us
    pallas_call x1, Pallas kernels, experts(): pl.pallas_call(functools.partial(expert_kernel, chunk, group), out_shape=...  4.76 us
    all_to_all x1, starting transfers between devices, exchange(): lax.all_to_all(chunks, 'ep', split_axis=0, concat_axis=0, tiled=True, axi...  3.6 us
    ppermute x2, waiting for transfers between devices, turn(): lax.ppermute(value, 'ep', [(i, i // group * group + (i % group + by) % gr...  3.31 us
    all_to_all x1, waiting for transfers between devices, exchange(): lax.all_to_all(chunks, 'ep', split_axis=0, concat_axis=0, tiled=True, axi...  2.94 us
  transfers between devices with their start and end apart: 3, of which 3 were waited for; matrix products, arithmetic and copies ran while one was open for 0% of the time, Pallas kernels for 16%

profile of v3, /device:TPU:0, one launch (start us, length us, event | category | flops | bytes accessed | tf_op | source)
XLA Modules:
  0.0 61.5 jit_solution(12821453110515642184)
XLA Ops:
  0.6 12.8 %mixer.1 = (bf16[128,1536]{1,0:T(8,128)(2,1)}, f32[24,2048]{1,0:T(8,128)}, f32[4,24,128]{2,1,0:T(8,128)}, f32[5,24,1024]{2,1,0:T(8,128)}) custom-call(s32[1]{0:T(128)} %bitcast.start, bf16[24,2048]{1,0:T(8,128)(2,1)} %tokens_in.1, f32[1,2048]{1,0:T(1,128)} %bitcast.17, f32[1,1024]{1,0:T(1,128)} %bitcast.21, f32[1,1024]{1,0:T(1,128)} %bitcast.22, ...), custom_call_target="tpu_custom_call" | custom-call | flops 24000000000 | bytes 30000000 | tf_op jit(solution)/shard_map/mixer/pallas_call | solution.py:291
  13.4 0.0 copy-start
  13.4 0.0 copy-start.1
  13.5 0.0 copy-start.2
  13.5 21.2 %all_to_all.10 = bf16[16,8,1536]{2,1,0:T(8,128)(2,1)S(1)} all-to-all(bf16[16,8,1536]{2,1,0:T(8,128)(2,1)} %bitcast.16), channel_id=1, replica_groups={{0,2,4,6,8,10,12,14,16,18,20,22,24,26,28,30},{1,3,5,7,9,11,13,15,17,19,..., dimensions={0} | all-to-all | bytes 786432 | tf_op jit(solution)/shard_map/all_to_all | solution.py:567
  34.7 0.0 collective-permute-start
  34.7 1.7 %collective-permute-done.refs_1_ = bf16[128,1536]{1,0:T(8,128)(2,1)S(1)} collective-permute-done((bf16[128,1536]{1,0:T(8,128)(2,1)S(1)}, bf16[128,1536]{1,0:T(8,128)(2,1)S(1)}, u32[]{:S(2)}, u32[]{:S(2)}) %collective-permute-start) | collective-permute-done | bytes 393248 | tf_op jit(solution)/shard_map/ppermute | solution.py:573
  36.4 0.0 copy-done
  36.4 0.0 copy-done.1
  36.4 0.0 copy-done.2
  36.5 4.8 %experts.1 = (bf16[128,1536]{1,0:T(8,128)(2,1)S(1)}, bf16[128,1536]{1,0:T(8,128)(2,1)S(1)}) custom-call(bf16[128,1536]{1,0:T(8,128)(2,1)S(1)} %bitcast.15, bf16[128,1536]{1,0:T(8,128)(2,1)S(1)} %collective-permute-done.refs_1_, bf16[2048,1536]{1,0:T(8,128)(2,1)S(1)} %copy-done, bf16[2048,1536]{1,0:T(8,128)(2,1)S(1)} %copy-done.1, ...), custom_call_target="tpu_custom_call" | custom-call | flops 3623878656 | bytes 18874368 | tf_op jit(solution)/shard_map/experts/pallas_call | solution.py:460
  41.2 0.2 collective-permute-start.1
  41.4 1.6 %collective-permute-done.1 = bf16[128,1536]{1,0:T(8,128)(2,1)S(1)} collective-permute-done((bf16[128,1536]{1,0:T(8,128)(2,1)S(1)}, bf16[128,1536]{1,0:T(8,128)(2,1)S(1)}, u32[]{:S(2)}, u32[]{:S(2)}) %collective-permute-start.1) | collective-permute-done | bytes 393248 | tf_op jit(solution)/shard_map/ppermute | solution.py:573
  43.0 0.8 %fusion = bf16[16,8,1536]{2,1,0:T(8,128)(2,1)} fusion(bf16[128,1536]{1,0:T(8,128)(2,1)S(1)} %collective-permute-done.1, bf16[128,1536]{1,0:T(8,128)(2,1)S(1)} %get-tuple-element.9), kind=kLoop, calls=%fused_computation.1 | loop fusion | flops 786432 | bytes 1179648 | tf_op jit(solution)/shard_map/reshape | solution.py:566
  43.9 3.6 %all-to-all-start.1 = ((bf16[16,8,1536]{2,1,0:T(8,128)(2,1)}), bf16[16,8,1536]{2,1,0:T(8,128)(2,1)S(1)}, u32[]{:S(2)}, u32[]{:S(2)}) async-start(bf16[16,8,1536]{2,1,0:T(8,128)(2,1)} %fusion), calls=%async_computation.1 | async-start | bytes 786432 | tf_op jit(solution)/shard_map/all_to_all | solution.py:567
  47.5 0.0 copy-start.3
  47.5 0.0 copy-start.4
  47.5 10.1 %update.1 = f32[24,16,64,64]{3,2,1,0:T(8,128)} custom-call(f32[24,16,64,64]{3,2,1,0:T(8,128)} %state.3, f32[5,24,1024]{2,1,0:T(8,128)} %get-tuple-element.13.terms_in), custom_call_target="tpu_custom_call" | custom-call | flops 16000000000 | bytes 26000000 | tf_op jit(solution)/shard_map/update/pallas_call | solution.py:391
  57.6 2.9 %all-to-all-done.1 = bf16[16,8,1536]{2,1,0:T(8,128)(2,1)S(1)} async-done(((bf16[16,8,1536]{2,1,0:T(8,128)(2,1)}), bf16[16,8,1536]{2,1,0:T(8,128)(2,1)S(1)}, u32[]{:S(2)}, u32[]{:S(2)}) %all-to-all-start.1) | async-done | bytes 393248 | tf_op jit(solution)/shard_map/all_to_all | solution.py:567
  60.5 0.0 copy-done.3
  60.5 0.0 copy-done.4
  60.5 1.0 %combine.1 = bf16[24,2048]{1,0:T(8,128)(2,1)} custom-call(bf16[128,1536]{1,0:T(8,128)(2,1)S(1)} %bitcast.13, f32[24,2048]{1,0:T(8,128)S(1)} %copy-done.3, f32[4,24,128]{2,1,0:T(8,128)S(1)} %copy-done.4), custom_call_target="tpu_custom_call" | custom-call | tf_op jit(solution)/shard_map/combine/pallas_call | solution.py:587
  (1 shorter events, 0.0 us)
Async XLA Ops:
  13.4 23.0 %copy-start = (bf16[2048,1536]{1,0:T(8,128)(2,1)S(1)}, bf16[2048,1536]{1,0:T(8,128)(2,1)}, u32[]{:S(2)}) copy-start(bf16[2048,1536]{1,0:T(8,128)(2,1)} %refs_2_.1) | copy-start | bytes 18874372
  13.4 23.0 %copy-start.1 = (bf16[2048,1536]{1,0:T(8,128)(2,1)S(1)}, bf16[2048,1536]{1,0:T(8,128)(2,1)}, u32[]{:S(2)}) copy-start(bf16[2048,1536]{1,0:T(8,128)(2,1)} %refs_3_.1) | copy-start | bytes 18874372
  13.5 23.0 %copy-start.2 = (bf16[1536,2048]{1,0:T(8,128)(2,1)S(1)}, bf16[1536,2048]{1,0:T(8,128)(2,1)}, u32[]{:S(2)}) copy-start(bf16[1536,2048]{1,0:T(8,128)(2,1)} %refs_4_.1) | copy-start | bytes 18874372
  34.7 1.7 %collective-permute-start = (bf16[128,1536]{1,0:T(8,128)(2,1)S(1)}, bf16[128,1536]{1,0:T(8,128)(2,1)S(1)}, u32[]{:S(2)}, u32[]{:S(2)}) collective-permute-start(bf16[128,1536]{1,0:T(8,128)(2,1)S(1)} %bitcast.14), channel_id=1, source_target_pairs={{0,1},{1,0},{2,3},{3,2},{4,5},{5,4},{6,7},{7,6},{8,9},{9,8},{10,11... | collective-permute-start | bytes 1179656 | tf_op jit(solution)/shard_map/ppermute | solution.py:573
  41.2 1.8 %collective-permute-start.1 = (bf16[128,1536]{1,0:T(8,128)(2,1)S(1)}, bf16[128,1536]{1,0:T(8,128)(2,1)S(1)}, u32[]{:S(2)}, u32[]{:S(2)}) collective-permute-start(bf16[128,1536]{1,0:T(8,128)(2,1)S(1)} %get-tuple-element.10), channel_id=1, source_target_pairs={{0,1},{1,0},{2,3},{3,2},{4,5},{5,4},{6,7},{7,6},{8,9},{9,8},{10,11... | collective-permute-start | bytes 1179656 | tf_op jit(solution)/shard_map/ppermute | solution.py:573
  43.9 16.7 %all-to-all-start.1 = ((bf16[16,8,1536]{2,1,0:T(8,128)(2,1)}), bf16[16,8,1536]{2,1,0:T(8,128)(2,1)S(1)}, u32[]{:S(2)}, u32[]{:S(2)}) async-start(bf16[16,8,1536]{2,1,0:T(8,128)(2,1)} %fusion), calls=%async_computation.1 | async-start | bytes 786432 | tf_op jit(solution)/shard_map/all_to_all | solution.py:567
  47.5 13.1 %copy-start.3 = (f32[24,2048]{1,0:T(8,128)S(1)}, f32[24,2048]{1,0:T(8,128)}, u32[]{:S(2)}) copy-start(f32[24,2048]{1,0:T(8,128)} %get-tuple-element.11.after) | copy-start | bytes 589828
  47.5 13.1 %copy-start.4 = (f32[4,24,128]{2,1,0:T(8,128)S(1)}, f32[4,24,128]{2,1,0:T(8,128)}, u32[]{:S(2)}) copy-start(f32[4,24,128]{2,1,0:T(8,128)} %get-tuple-element.12.combine) | copy-start | bytes 147460

commit v4 on v3

--- a/solution.py
+++ b/solution.py
@@ -29,10 +29,6 @@
 
 def dot(a, b):
     return jnp.dot(a, b, preferred_element_type=F32)
-
-
-def dot_t(a, b):
-    return lax.dot_general(a, b, (((0,), (0,)), ((), ())), preferred_element_type=F32)
 
 
 def head_sums(x):
@@ -409,6 +405,39 @@
     )(pin(state), pin(terms))
 
 
+def unpack_tables():
+    shape = (EXPERTS * CAP_DEV, EXPERTS * ROWS)
+    source, c, column = iota(shape, 0) // CAP_DEV, iota(shape, 0) % CAP_DEV, iota(shape, 1)
+    tables = [jnp.where(column == source * ROWS + c, 1.0, 0.0).astype(BF16)]
+    for j in range(SPLIT):
+        here = (column == source * ROWS + CAP_DEV + c // SPLIT) & (c % SPLIT == j)
+        tables.append(jnp.where(here, 1.0, 0.0).astype(BF16))
+    return tables
+
+
+def unpack(tables, value, out):
+    piece = value.shape[1] // SPLIT
+    out[:, : SPLIT * piece] = dot(tables[0], value).astype(BF16)
+    out[:, SPLIT * piece :] = sum(
+        dot(tables[1 + j], value[:, j * piece : (j + 1) * piece]) for j in range(SPLIT)
+    ).astype(BF16)
+
+
+def unpack_own(value):
+    rows, width = EXPERTS * CAP_DEV, value.shape[1] * (SPLIT + 1) // SPLIT
+    return pl.pallas_call(
+        lambda source, out: unpack(unpack_tables(), source[...], out),
+        out_shape=jax.ShapeDtypeStruct((rows, width), BF16),
+        in_specs=[VMEM],
+        out_specs=VMEM,
+        compiler_params=pltpu.CompilerParams(vmem_limit_bytes=4 * 1024 * 1024),
+        cost_estimate=pl.CostEstimate(
+            flops=2_000_000_000, bytes_accessed=800_000, transcendentals=0
+        ),
+        name="unpack",
+    )(value)
+
+
 def expert_kernel(chunk, group, *refs):
     received = refs[:group]
     gate, up, down = refs[group : group + 3]
@@ -420,19 +449,11 @@
     slots = EXPERTS * CAP_DEV
     packed_rows = EXPERTS * ROWS
 
-    source, c = iota((slots, packed_rows), 0) // CAP_DEV, iota((slots, packed_rows), 0) % CAP_DEV
-    column = iota((slots, packed_rows), 1)
-    tables = [jnp.where(column == source * ROWS + c, 1.0, 0.0).astype(BF16)]
-    for j in range(SPLIT):
-        here = (column == source * ROWS + CAP_DEV + c // SPLIT) & (c % SPLIT == j)
-        tables.append(jnp.where(here, 1.0, 0.0).astype(BF16))
-    for m in range(group):
+    x_buf[:slots] = received[0][...]
+    tables = unpack_tables()
+    for m in range(1, group):
         at = slice(m * slots, (m + 1) * slots)
-        value = received[m][...]
-        x_buf[at, : SPLIT * piece] = dot(tables[0], value).astype(BF16)
-        x_buf[at, SPLIT * piece :] = sum(
-            dot(tables[1 + j], value[:, j * piece : (j + 1) * piece]) for j in range(SPLIT)
-        ).astype(BF16)
+        unpack(tables, received[m][...], x_buf.at[at])
 
     for i in range(steps):
         at = slice(i * chunk, (i + 1) * chunk)
@@ -443,16 +464,22 @@
         y = dot(h, down[at])
         acc[...] = y if i == 0 else acc[...] + y
 
+    source, c = iota((packed_rows, slots), 1) // CAP_DEV, iota((packed_rows, slots), 1) % CAP_DEV
+    column = iota((packed_rows, slots), 0)
+    tables = [jnp.where(column == source * ROWS + c, 1.0, 0.0).astype(BF16)]
+    for j in range(SPLIT):
+        here = (column == source * ROWS + CAP_DEV + c // SPLIT) & (c % SPLIT == j)
+        tables.append(jnp.where(here, 1.0, 0.0).astype(BF16))
     for m in range(group):
         y = acc[m * slots : (m + 1) * slots].astype(BF16)
         last = y[:, SPLIT * piece :]
         for j in range(SPLIT):
             results[m][:, j * piece : (j + 1) * piece] = (
-                dot_t(tables[0], y[:, j * piece : (j + 1) * piece]) + dot_t(tables[1 + j], last)
+                dot(tables[0], y[:, j * piece : (j + 1) * piece]) + dot(tables[1 + j], last)
             ).astype(BF16)
 
 
-def experts(received, gate, up, down):
+def experts(own, received, gate, up, down):
     group = len(received)
     width, hidden = gate.shape
     chunk = next(c for c in (768, 384, 128) if hidden % c == 0)
@@ -471,7 +498,7 @@
             flops=6 * rows * width * hidden, bytes_accessed=6 * width * hidden, transcendentals=0
         ),
         name="experts",
-    )(*received, gate, up, down)
+    )(own, *received[1:], gate, up, down)
 
 
 def window(value):
@@ -579,7 +606,7 @@
     own = exchange(window(packed))
     new_state = update(state, terms)
     received = (own,) + tuple(turn(own, by) for by in range(1, group))
-    results = experts(received, expert_gate, expert_up, expert_down)
+    results = experts(unpack_own(own), received, expert_gate, expert_up, expert_down)
     total = results[0].astype(F32)
     for by in range(1, group):
         total = total + turn(results[by], group - by).astype(F32)

time: 61.7 us -> 61.7 us (level)
  transfers between devices with their start and end apart: 3 -> 3, of which waited for: 3 -> 3; matrix products, arithmetic and copies ran while one was open for 0% -> 0% of each run, Pallas kernels for 16% -> 17%
where the time goes in v4:
time: 61.7 us; the launch traced here: 61.5 us
  Pallas kernels  28.8 us (47%)
  blocking collectives  21.2 us (34%)
  waiting for transfers between devices  5.94 us (10%)
  starting transfers between devices  3.8 us (6%)
  other arithmetic  0.83 us (1%)
  between operations  0.81 us (1%)
    all_to_all x1, blocking collectives, exchange(): lax.all_to_all(chunks, 'ep', split_axis=0, concat_axis=0, tiled=True, axi...  21.2 us
    pallas_call x1, Pallas kernels, mixer(): pl.pallas_call(mixer_kernel, out_shape=(pltpu.HBM((EXPERTS * ROWS, width...  12.8 us
    pallas_call x1, Pallas kernels, update(): pl.pallas_call(update_kernel, out_shape=jax.ShapeDtypeStruct(state.shape,...  10.1 us
    pallas_call x1, Pallas kernels, experts(): pl.pallas_call(functools.partial(expert_kernel, chunk, group), out_shape=...  4.63 us
    all_to_all x1, starting transfers between devices, exchange(): lax.all_to_all(chunks, 'ep', split_axis=0, concat_axis=0, tiled=True, axi...  3.6 us
    ppermute x2, waiting for transfers between devices, turn(): lax.ppermute(value, 'ep', [(i, i // group * group + (i % group + by) % gr...  3 us
    all_to_all x1, waiting for transfers between devices, exchange(): lax.all_to_all(chunks, 'ep', split_axis=0, concat_axis=0, tiled=True, axi...  2.94 us
  transfers between devices with their start and end apart: 3, of which 3 were waited for; matrix products, arithmetic and copies ran while one was open for 0% of the time, Pallas kernels for 17%

profile of v4, /device:TPU:0, one launch (start us, length us, event | category | flops | bytes accessed | tf_op | source)
XLA Modules:
  0.0 61.5 jit_solution(5034297379651892606)
XLA Ops:
  0.6 12.8 %mixer.1 = (bf16[128,1536]{1,0:T(8,128)(2,1)}, f32[24,2048]{1,0:T(8,128)}, f32[4,24,128]{2,1,0:T(8,128)}, f32[5,24,1024]{2,1,0:T(8,128)}) custom-call(s32[1]{0:T(128)} %bitcast.start, bf16[24,2048]{1,0:T(8,128)(2,1)} %tokens_in.1, f32[1,2048]{1,0:T(1,128)} %bitcast.23, f32[1,1024]{1,0:T(1,128)} %bitcast.27, f32[1,1024]{1,0:T(1,128)} %bitcast.28, ...), custom_call_target="tpu_custom_call" | custom-call | flops 24000000000 | bytes 30000000 | tf_op jit(solution)/shard_map/mixer/pallas_call | solution.py:287
  13.4 0.0 slice-start
  13.4 0.0 slice-start.2
  13.5 0.0 slice-start.4
  13.5 0.0 slice-start.1
  13.5 0.0 slice-start.3
  13.5 0.0 slice-start.5
  13.5 21.2 %all_to_all.10 = bf16[16,8,1536]{2,1,0:T(8,128)(2,1)S(1)} all-to-all(bf16[16,8,1536]{2,1,0:T(8,128)(2,1)} %bitcast.22), channel_id=1, replica_groups={{0,2,4,6,8,10,12,14,16,18,20,22,24,26,28,30},{1,3,5,7,9,11,13,15,17,19,..., dimensions={0} | all-to-all | bytes 786432 | tf_op jit(solution)/shard_map/all_to_all | solution.py:594
  34.7 0.0 collective-permute-start
  34.8 0.3 unpack.1.refs_0_
  35.1 1.4 %collective-permute-done.refs_1_ = bf16[128,1536]{1,0:T(8,128)(2,1)S(1)} collective-permute-done((bf16[128,1536]{1,0:T(8,128)(2,1)S(1)}, bf16[128,1536]{1,0:T(8,128)(2,1)S(1)}, u32[]{:S(2)}, u32[]{:S(2)}) %collective-permute-start) | collective-permute-done | bytes 393248 | tf_op jit(solution)/shard_map/ppermute | solution.py:600
  36.5 0.0 slice-done
  36.5 0.0 slice-done.2
  36.5 0.0 slice-done.4
  36.5 0.0 slice-done.1
  36.5 0.0 slice-done.3
  36.5 0.0 slice-done.5
  36.5 4.6 %experts.1 = (bf16[128,1536]{1,0:T(8,128)(2,1)S(1)}, bf16[128,1536]{1,0:T(8,128)(2,1)S(1)}) custom-call(bf16[96,2048]{1,0:T(8,128)(2,1)S(1)} %unpack.1.refs_0_, bf16[128,1536]{1,0:T(8,128)(2,1)S(1)} %collective-permute-done.refs_1_, bf16[2048,1536]{1,0:T(8,128)(2,1)S(1)} %bitcast.14, bf16[2048,1536]{1,0:T(8,128)(2,1)S(1)} %bitcast.16, ...), custom_call_target="tpu_custom_call" | custom-call | flops 3623878656 | bytes 18874368 | tf_op jit(solution)/shard_map/experts/pallas_call | solution.py:487
  41.2 0.2 collective-permute-start.1
  41.4 1.6 %collective-permute-done.1 = bf16[128,1536]{1,0:T(8,128)(2,1)S(1)} collective-permute-done((bf16[128,1536]{1,0:T(8,128)(2,1)S(1)}, bf16[128,1536]{1,0:T(8,128)(2,1)S(1)}, u32[]{:S(2)}, u32[]{:S(2)}) %collective-permute-start.1) | collective-permute-done | bytes 393248 | tf_op jit(solution)/shard_map/ppermute | solution.py:600
  43.0 0.8 %fusion = bf16[16,8,1536]{2,1,0:T(8,128)(2,1)} fusion(bf16[128,1536]{1,0:T(8,128)(2,1)S(1)} %collective-permute-done.1, bf16[128,1536]{1,0:T(8,128)(2,1)S(1)} %get-tuple-element.9), kind=kLoop, calls=%fused_computation.1 | loop fusion | flops 786432 | bytes 1179648 | tf_op jit(solution)/shard_map/reshape | solution.py:593
  43.8 3.6 %all-to-all-start.1 = ((bf16[16,8,1536]{2,1,0:T(8,128)(2,1)}), bf16[16,8,1536]{2,1,0:T(8,128)(2,1)S(1)}, u32[]{:S(2)}, u32[]{:S(2)}) async-start(bf16[16,8,1536]{2,1,0:T(8,128)(2,1)} %fusion), calls=%async_computation.1 | async-start | bytes 786432 | tf_op jit(solution)/shard_map/all_to_all | solution.py:594
  47.4 0.0 copy-start
  47.4 0.0 copy-start.1
  47.4 10.1 %update.1 = f32[24,16,64,64]{3,2,1,0:T(8,128)} custom-call(f32[24,16,64,64]{3,2,1,0:T(8,128)} %state.3, f32[5,24,1024]{2,1,0:T(8,128)} %get-tuple-element.13.terms_in), custom_call_target="tpu_custom_call" | custom-call | flops 16000000000 | bytes 26000000 | tf_op jit(solution)/shard_map/update/pallas_call | solution.py:387
  57.5 2.9 %all-to-all-done.1 = bf16[16,8,1536]{2,1,0:T(8,128)(2,1)S(1)} async-done(((bf16[16,8,1536]{2,1,0:T(8,128)(2,1)}), bf16[16,8,1536]{2,1,0:T(8,128)(2,1)S(1)}, u32[]{:S(2)}, u32[]{:S(2)}) %all-to-all-start.1) | async-done | bytes 393248 | tf_op jit(solution)/shard_map/all_to_all | solution.py:594
  60.5 0.0 copy-done
  60.5 0.0 copy-done.1
  60.5 1.0 %combine.1 = bf16[24,2048]{1,0:T(8,128)(2,1)} custom-call(bf16[128,1536]{1,0:T(8,128)(2,1)S(1)} %bitcast.19, f32[24,2048]{1,0:T(8,128)S(1)} %copy-done, f32[4,24,128]{2,1,0:T(8,128)S(1)} %copy-done.1), custom_call_target="tpu_custom_call" | custom-call | tf_op jit(solution)/shard_map/combine/pallas_call | solution.py:614
  (4 shorter events, 0.0 us)
Async XLA Ops:
  13.4 23.0 %slice-start = ((s8[6291456]{0:T(1024)(128)(4,1)}), s8[4194304]{0:T(1024)(128)(4,1)S(1)}, s32[]{:S(2)}) async-start(s8[6291456]{0:T(1024)(128)(4,1)} %bitcast.13), calls=%async_computation.2 | async-start | bytes 8388608
  13.4 23.0 %slice-start.2 = ((s8[6291456]{0:T(1024)(128)(4,1)}), s8[4194304]{0:T(1024)(128)(4,1)S(1)}, s32[]{:S(2)}) async-start(s8[6291456]{0:T(1024)(128)(4,1)} %bitcast.15), calls=%async_computation.4 | async-start | bytes 8388608
  13.5 23.0 %slice-start.4 = ((s8[6291456]{0:T(1024)(128)(4,1)}), s8[4194304]{0:T(1024)(128)(4,1)S(1)}, s32[]{:S(2)}) async-start(s8[6291456]{0:T(1024)(128)(4,1)} %bitcast.17), calls=%async_computation.6 | async-start | bytes 8388608
  13.5 23.0 %slice-start.1 = ((s8[6291456]{0:T(1024)(128)(4,1)}), s8[2097152]{0:T(1024)(128)(4,1)S(1)}, s32[]{:S(2)}) async-start(s8[6291456]{0:T(1024)(128)(4,1)} %bitcast.13), calls=%async_computation.3 | async-start | bytes 4194304
  13.5 23.0 %slice-start.3 = ((s8[6291456]{0:T(1024)(128)(4,1)}), s8[2097152]{0:T(1024)(128)(4,1)S(1)}, s32[]{:S(2)}) async-start(s8[6291456]{0:T(1024)(128)(4,1)} %bitcast.15), calls=%async_computation.5 | async-start | bytes 4194304
  13.5 23.0 %slice-start.5 = ((s8[6291456]{0:T(1024)(128)(4,1)}), s8[2097152]{0:T(1024)(128)(4,1)S(1)}, s32[]{:S(2)}) async-start(s8[6291456]{0:T(1024)(128)(4,1)} %bitcast.17), calls=%async_computation.7 | async-start | bytes 4194304
  34.7 1.7 %collective-permute-start = (bf16[128,1536]{1,0:T(8,128)(2,1)S(1)}, bf16[128,1536]{1,0:T(8,128)(2,1)S(1)}, u32[]{:S(2)}, u32[]{:S(2)}) collective-permute-start(bf16[128,1536]{1,0:T(8,128)(2,1)S(1)} %bitcast.20), channel_id=1, source_target_pairs={{0,1},{1,0},{2,3},{3,2},{4,5},{5,4},{6,7},{7,6},{8,9},{9,8},{10,11... | collective-permute-start | bytes 1179656 | tf_op jit(solution)/shard_map/ppermute | solution.py:600
  41.2 1.8 %collective-permute-start.1 = (bf16[128,1536]{1,0:T(8,128)(2,1)S(1)}, bf16[128,1536]{1,0:T(8,128)(2,1)S(1)}, u32[]{:S(2)}, u32[]{:S(2)}) collective-permute-start(bf16[128,1536]{1,0:T(8,128)(2,1)S(1)} %get-tuple-element.10), channel_id=1, source_target_pairs={{0,1},{1,0},{2,3},{3,2},{4,5},{5,4},{6,7},{7,6},{8,9},{9,8},{10,11... | collective-permute-start | bytes 1179656 | tf_op jit(solution)/shard_map/ppermute | solution.py:600
  43.8 16.7 %all-to-all-start.1 = ((bf16[16,8,1536]{2,1,0:T(8,128)(2,1)}), bf16[16,8,1536]{2,1,0:T(8,128)(2,1)S(1)}, u32[]{:S(2)}, u32[]{:S(2)}) async-start(bf16[16,8,1536]{2,1,0:T(8,128)(2,1)} %fusion), calls=%async_computation.1 | async-start | bytes 786432 | tf_op jit(solution)/shard_map/all_to_all | solution.py:594
  47.4 13.1 %copy-start = (f32[24,2048]{1,0:T(8,128)S(1)}, f32[24,2048]{1,0:T(8,128)}, u32[]{:S(2)}) copy-start(f32[24,2048]{1,0:T(8,128)} %get-tuple-element.11.after) | copy-start | bytes 589828
  47.4 13.1 %copy-start.1 = (f32[4,24,128]{2,1,0:T(8,128)S(1)}, f32[4,24,128]{2,1,0:T(8,128)}, u32[]{:S(2)}) copy-start(f32[4,24,128]{2,1,0:T(8,128)} %get-tuple-element.12.combine) | copy-start | bytes 147460
